TPU v7x, 32 devices: a whole 2x2x4 slice. The times are simulated.
32 devices in a mesh: tp: 8 (over z, core), dp: 4 (over y, x).
Axes of the slice: x: 2, y: 2, z: 4, core: 2. Of those that a mesh axis runs over, the one named last changes fastest.
Arguments:
- tokens: bfloat16 [32, 4096], P('tp', 'dp'), may hold values from -6 to 6
- norm_gain: bfloat16 [2, 4096], P(None, 'dp'), may hold values from 0.099609375 to 1.8984375
- w_query: bfloat16 [2, 4096, 1024], P(None, 'dp', 'tp'), may hold values from -0.09375 to 0.09375
- w_key: bfloat16 [2, 4096, 1024], P(None, 'dp', 'tp'), may hold values from -0.09375 to 0.09375
- w_value: bfloat16 [2, 4096, 1024], P(None, 'dp', 'tp'), may hold values from -0.09375 to 0.09375
- w_outgate: bfloat16 [2, 4096, 1024], P(None, 'dp', 'tp'), may hold values from -0.09375 to 0.09375
- w_gates: bfloat16 [2, 4096, 16], P(None, 'dp'), may hold values from -0.09375 to 0.09375
- gate_bias: float32 [2, 2, 8], P(None, None, 'tp'), may hold values from -1 to 5
- w_out: bfloat16 [2, 1024, 4096], P(None, 'tp', 'dp'), may hold values from -0.1875 to 0.1875
- memory: float32 [2, 32, 8, 128, 128], P(None, 'dp', 'tp'), may hold values from -6 to 6
- normalizer: float32 [2, 32, 8, 128], P(None, 'dp', 'tp'), may hold values from -3 to 3
- stabilizer: float32 [2, 32, 8], P(None, 'dp', 'tp'), may hold values from -8 to 300, as said below
Outputs:
- mixed: bfloat16 [32, 4096], P('tp', 'dp')
- new_memory: float32 [2, 32, 8, 128, 128], P(None, 'dp', 'tp')
- new_normalizer: float32 [2, 32, 8, 128], P(None, 'dp', 'tp')
- new_stabilizer: float32 [2, 32, 8], P(None, 'dp', 'tp')
Inputs may be any that keep to these rules, and one draw needn't show every extreme that they name: `stabilizer`: lies between -8 and 8, except that some entries may be as large as 300.
All inputs are finite; a program needn't handle non-finite values.
Results may differ from a plain program's by a relative error of at most 0.04.
Values may be sent and summed in bfloat16 or wider, within the bound.
No kernel may reach another device: no remote copies, remote signals or barrier semaphores. Data moves between devices by JAX's collectives and lax.ppermute only.
A program may use at most 64 MiB of HBM per device.

v0:
```python
import jax
import jax.numpy as jnp
from jax import lax
from jax.sharding import PartitionSpec as P

D = 4096
HEAD_SIZE = 128


epsilon = 1e-06


def cell_update(query, key_rows, value_rows, input_pre, forget_pre, memory, normalizer, stabilizer):
    batch_size = query.shape[0]
    head_count = input_pre.shape[1]
    query_float = query.astype(jnp.float32).reshape(batch_size, head_count, -1)
    key_float = key_rows.astype(jnp.float32).reshape(
        batch_size, head_count, -1
    ) * query_float.shape[2] ** (-0.5)
    value_float = value_rows.astype(jnp.float32).reshape(batch_size, head_count, -1)
    carried = jax.nn.log_sigmoid(forget_pre) + stabilizer
    new_max = jnp.maximum(carried, input_pre)
    keep_factor = jnp.exp(carried - new_max)
    write_factor = jnp.exp(input_pre - new_max)
    new_memory = (
        keep_factor[:, :, None, None] * memory
        + write_factor[:, :, None, None] * value_float[:, :, :, None] * key_float[:, :, None, :]
    )
    new_normalizer = keep_factor[:, :, None] * normalizer + write_factor[:, :, None] * key_float
    numerator = jnp.sum(new_memory * query_float[:, :, None, :], axis=3)
    denominator = jnp.sum(new_normalizer * query_float, axis=2)
    floor_value = jnp.maximum(jnp.abs(denominator), jnp.exp(-new_max))
    readout = numerator / jnp.maximum(floor_value, 1.0)[:, :, None]
    return (readout.reshape(batch_size, -1), new_memory, new_normalizer, new_max)


def finish_split(partial_out, wide_rows):
    summed = lax.psum_scatter(partial_out, "tp", scatter_dimension=0, tiled=True)
    own_rows = lax.dynamic_slice_in_dim(
        wide_rows, lax.axis_index("tp") * summed.shape[0], summed.shape[0], 0
    )
    return (own_rows + summed).astype(jnp.bfloat16)


def body(
    tokens,
    norm_gain,
    w_query,
    w_key,
    w_value,
    w_outgate,
    w_gates,
    gate_bias,
    w_out,
    memory,
    normalizer,
    stabilizer,
):
    heads_here = w_query.shape[2] // HEAD_SIZE
    seq_here = memory.shape[1]
    all_heads = w_gates.shape[2] // 2
    head_first = lax.axis_index("tp") * heads_here
    seq_first = lax.axis_index("dp") * seq_here
    current = tokens
    gathered = None
    memories = []
    normalizers = []
    maxima = []
    for layer_index in range(2):
        if gathered is None:
            gathered = lax.all_gather(current, "tp", axis=0, tiled=True)
        wide_rows = gathered.astype(jnp.float32)
        square_part = jnp.sum(wide_rows * wide_rows, axis=1)
        scaled = (wide_rows * norm_gain[layer_index].astype(jnp.float32)[None, :]).astype(
            jnp.bfloat16
        )
        gate_weight = w_gates[layer_index]
        own_gates = jnp.concatenate(
            [
                lax.dynamic_slice_in_dim(gate_weight, head_first, heads_here, 1),
                lax.dynamic_slice_in_dim(gate_weight, all_heads + head_first, heads_here, 1),
            ],
            axis=1,
        )
        term_query = jnp.dot(scaled, w_query[layer_index], preferred_element_type=jnp.float32)
        term_key = jnp.dot(scaled, w_key[layer_index], preferred_element_type=jnp.float32)
        term_value = jnp.dot(scaled, w_value[layer_index], preferred_element_type=jnp.float32)
        term_outgate = jnp.dot(scaled, w_outgate[layer_index], preferred_element_type=jnp.float32)
        term_gates = jnp.dot(scaled, own_gates, preferred_element_type=jnp.float32)
        square_all = lax.psum(square_part, "dp")
        square_own = lax.dynamic_slice_in_dim(square_all, seq_first, seq_here, 0)
        sum_query, sum_key, sum_value, sum_outgate, sum_gates = (
            lax.psum_scatter(term_query, "dp", scatter_dimension=0, tiled=True),
            lax.psum_scatter(term_key, "dp", scatter_dimension=0, tiled=True),
            lax.psum_scatter(term_value, "dp", scatter_dimension=0, tiled=True),
            lax.psum_scatter(term_outgate, "dp", scatter_dimension=0, tiled=True),
            lax.psum_scatter(term_gates, "dp", scatter_dimension=0, tiled=True),
        )
        inv_scale = lax.rsqrt(square_own / D + epsilon)[:, None]
        query = (sum_query * inv_scale).astype(jnp.bfloat16)
        key_rows = (sum_key * inv_scale).astype(jnp.bfloat16)
        value_rows = (sum_value * inv_scale).astype(jnp.bfloat16)
        outgate = (sum_outgate * inv_scale).astype(jnp.bfloat16)
        gate_pre = sum_gates * inv_scale
        bias_here = gate_bias[layer_index]
        input_pre = gate_pre[:, :heads_here] + bias_here[0][None, :]
        forget_pre = gate_pre[:, heads_here:] + bias_here[1][None, :]
        readout, new_memory, new_normalizer, new_max = cell_update(
            query,
            key_rows,
            value_rows,
            input_pre,
            forget_pre,
            memory[layer_index],
            normalizer[layer_index],
            stabilizer[layer_index],
        )
        gated = (jax.nn.sigmoid(outgate.astype(jnp.float32)) * readout).astype(jnp.bfloat16)
        out_weight = w_out[layer_index]
        partial_out = jnp.dot(
            lax.all_gather(gated, "dp", axis=0, tiled=True),
            out_weight,
            preferred_element_type=jnp.float32,
        )
        if layer_index == 0:
            summed = lax.psum(partial_out, "tp")
            gathered = (wide_rows + summed).astype(jnp.bfloat16)
        else:
            current = finish_split(partial_out, wide_rows)
        memories.append(new_memory)
        normalizers.append(new_normalizer)
        maxima.append(new_max)
    return (current, jnp.stack(memories), jnp.stack(normalizers), jnp.stack(maxima))


def solution(mesh):
    placed = (
        P("tp", "dp"),
        P(None, "dp"),
        P(None, "dp", "tp"),
        P(None, "dp", "tp"),
        P(None, "dp", "tp"),
        P(None, "dp", "tp"),
        P(None, "dp", None),
        P(None, None, "tp"),
        P(None, "tp", "dp"),
        P(None, "dp", "tp", None, None),
        P(None, "dp", "tp", None),
        P(None, "dp", "tp"),
    )
    return jax.shard_map(
        body,
        mesh=mesh,
        in_specs=placed,
        out_specs=(
            P("tp", "dp"),
            P(None, "dp", "tp", None, None),
            P(None, "dp", "tp", None),
            P(None, "dp", "tp"),
        ),
        check_vma=False,
    )
```

profile of v0, /device:TPU:0, one launch (start us, length us, event | category | flops | bytes accessed | tf_op | source)
XLA Modules:
  0.0 269.4 jit_solution(6725401215718095154)
XLA Ops:
  7.2 0.8 slice_convert_fusion
  8.0 15.9 %all-gather = bf16[8,4,1024]{2,1,0:T(4,128)(2,1)S(1)} all-gather(bf16[1,4,1024]{2,1,0:T(4,128)(2,1)} %bitcast.146), channel_id=1, replica_groups=mesh['tp'=8,'dp'=4] {'tp'}, dimensions={0}, use_global_device_ids=true | all-gather | bytes 73728 | tf_op jit(solution)/shard_map/all_gather | solution.py:71
  24.6 1.7 fusion.18
  26.3 0.8 fusion.20
  27.1 0.8 fusion.22
  27.9 1.8 fusion.24
  29.7 0.7 fusion.42
  32.4 40.8 %all-reduce.24.cloned.1.call-done = (f32[32,128]{1,0:T(8,128)}, f32[32]{0:T(128)}, f32[32,128]{1,0:T(8,128)}, f32[32,128]{1,0:T(8,128)}, f32[32,2]{0,1:T(2,128)}, /*index=5*/f32[32,128]{1,0:T(8,128)}) async-done(((f32[32,128]{1,0:T(8,128)}, f32[32]{0:T(128)}, f32[32,128]{1,0:T(8,128)}, f32[32,128]{1,0:T(8,128)}, f32[32,2]{0,1:T(2,128)}, /*index=5*/f32[32,128]{1,0:T(8,128)}), (f32[32,128]{1,0:T(8,128)}, ...) | async-done | bytes 65936
  73.2 0.7 add_rsqrt_fusion.1
  74.0 0.7 fusion.62
  74.7 1.4 broadcast_multiply_fusion.1
  76.1 0.8 fusion.59
  76.8 0.9 multiply_reduce_fusion.3
  78.1 0.8 multiply_convert_fusion.3
  78.9 8.9 %all_gather.10 = bf16[32,128]{1,0:T(8,128)(2,1)S(1)} all-gather(bf16[8,128]{1,0:T(8,128)(2,1)S(1)} %multiply_convert_fusion.3), channel_id=1, replica_groups=mesh['tp'=8,'dp'=4] {'dp'}, dimensions={0}, use_global_device_ids=true | all-gather | bytes 10240 | tf_op jit(solution)/shard_map/all_gather | solution.py:121
  87.8 0.8 fusion.16
  88.7 55.4 %all-reduce.18.cloned.1.call-done = f32[32,1024]{1,0:T(8,128)} async-done(((f32[32,1024]{1,0:T(8,128)}), f32[32,1024]{1,0:T(8,128)}) %all-reduce.18.cloned.1.call-update) | async-done | bytes 131088 | tf_op jit(solution)/shard_map/psum | solution.py:126
  144.1 1.5 multiply_reduce_fusion
  145.7 0.8 fusion.8
  146.5 0.8 fusion.10
  147.2 0.8 fusion.12
  148.0 0.8 fusion.14
  151.4 38.9 %all-reduce.22.cloned.1.call-done = (f32[32,128]{1,0:T(8,128)}, f32[32]{0:T(128)}, f32[32,128]{1,0:T(8,128)}, f32[32,128]{1,0:T(8,128)}, f32[32,2]{0,1:T(2,128)}, /*index=5*/f32[32,128]{1,0:T(8,128)}) async-done(((f32[32,128]{1,0:T(8,128)}, f32[32]{0:T(128)}, f32[32,128]{1,0:T(8,128)}, f32[32,128]{1,0:T(8,128)}, f32[32,2]{0,1:T(2,128)}, /*index=5*/f32[32,128]{1,0:T(8,128)}), (f32[32,128]{1,0:T(8,128)}, ...) | async-done | bytes 65936
  191.8 1.3 broadcast_multiply_fusion
  193.1 0.8 fusion.58
  193.9 0.9 multiply_reduce_fusion.2
  195.6 0.8 multiply_convert_fusion.2
  196.3 8.9 %all_gather.11 = bf16[32,128]{1,0:T(8,128)(2,1)S(1)} all-gather(bf16[8,128]{1,0:T(8,128)(2,1)S(1)} %multiply_convert_fusion.2), channel_id=1, replica_groups=mesh['tp'=8,'dp'=4] {'dp'}, dimensions={0}, use_global_device_ids=true | all-gather | bytes 10240 | tf_op jit(solution)/shard_map/all_gather | solution.py:121
  205.2 0.8 fusion.6
  206.7 1.1 pad_maximum_fusion
  208.3 53.2 %all-reduce.20.cloned.1.call-done = f32[32,1024]{1,0:T(8,128)} async-done(((f32[32,1024]{1,0:T(8,128)}), f32[32,1024]{1,0:T(8,128)}) %all-reduce.20.cloned.1.call-update) | async-done | bytes 131088
  261.5 1.4 fusion.37
  (57 shorter events, 8.0 us)
Async XLA Ops:
  7.2 19.1 %copy-start.2 = (bf16[2,1024,128]{2,1,0:T(8,128)(2,1)S(1)}, bf16[2,1024,128]{2,1,0:T(8,128)(2,1)}, u32[]{:S(2)}) copy-start(bf16[2,1024,128]{2,1,0:T(8,128)(2,1)} %param.15) | copy-start | bytes 1572868
  7.2 66.0 %all-reduce.24.cloned.1.call-start = ((), (), s32[]{:S(2)}) async-start(), calls=%async_computation.3 | async-start | bytes 134144
  23.9 3.2 %copy-start.3 = (bf16[2,1024,128]{2,1,0:T(8,128)(2,1)S(1)}, bf16[2,1024,128]{2,1,0:T(8,128)(2,1)}, u32[]{:S(2)}) copy-start(bf16[2,1024,128]{2,1,0:T(8,128)(2,1)} %param.16) | copy-start | bytes 1572868
  23.9 5.7 %copy-start.6 = (bf16[2,1024,16]{1,2,0:T(8,128)(2,1)S(1)}, bf16[2,1024,16]{1,2,0:T(8,128)(2,1)}, u32[]{:S(2)}) copy-start(bf16[2,1024,16]{1,2,0:T(8,128)(2,1)} %param.18) | copy-start | bytes 196612
  23.9 53.8 %copy-start = (f32[2,8,1,128,128]{4,3,2,1,0:T(8,128)S(1)}, f32[2,8,1,128,128]{4,3,2,1,0:T(8,128)}, u32[]{:S(2)}) copy-start(f32[2,8,1,128,128]{4,3,2,1,0:T(8,128)} %param.21) | copy-start | bytes 3145732
  27.8 2.6 copy-start.13
  27.9 3.9 %copy-start.8 = (f32[2,2,1]{1,2,0:T(1,128)S(1)}, f32[2,2,1]{1,2,0:T(1,128)}, u32[]{:S(2)}) copy-start(f32[2,2,1]{1,2,0:T(1,128)} %param.19) | copy-start | bytes 52
  27.9 46.8 %copy-start.9 = (f32[2,8,1]{1,2,0:T(1,128)S(1)}, f32[2,8,1]{1,2,0:T(1,128)}, u32[]{:S(2)}) copy-start(f32[2,8,1]{1,2,0:T(1,128)} %param.23) | copy-start | bytes 196
  27.9 48.2 %copy-start.7 = (f32[2,8,1,128]{3,2,1,0:T(1,128)S(1)}, f32[2,8,1,128]{3,2,1,0:T(1,128)}, u32[]{:S(2)}) copy-start(f32[2,8,1,128]{3,2,1,0:T(1,128)} %param.22) | copy-start | bytes 24580
  29.6 58.1 %copy-start.5 = (bf16[2,128,1024]{2,1,0:T(8,128)(2,1)S(1)}, bf16[2,128,1024]{2,1,0:T(8,128)(2,1)}, u32[]{:S(2)}) copy-start(bf16[2,128,1024]{2,1,0:T(8,128)(2,1)} %param.20) | copy-start | bytes 1572868
  30.4 113.7 %all-reduce.18.cloned.1.call-start = ((), (), s32[]{:S(2)}) async-start(), calls=%async_computation | async-start | bytes 262144 | tf_op jit(solution)/shard_map/psum | solution.py:126
  87.8 57.9 %copy-start.1 = (bf16[2,1024,128]{2,1,0:T(8,128)(2,1)S(1)}, bf16[2,1024,128]{2,1,0:T(8,128)(2,1)}, u32[]{:S(2)}) copy-start(bf16[2,1024,128]{2,1,0:T(8,128)(2,1)} %param.14) | copy-start | bytes 1572868
  88.6 101.7 %all-reduce.22.cloned.1.call-start = ((), (), s32[]{:S(2)}) async-start(), calls=%async_computation.2 | async-start | bytes 134144
  145.7 2.3 copy-start.4
  149.5 112.0 %all-reduce.20.cloned.1.call-start = ((), (), s32[]{:S(2)}) async-start(), calls=%async_computation.1 | async-start | bytes 262144
  149.5 0.7 copy-start.12
  190.4 0.7 copy-start.11
  191.1 0.6 copy-start.10
Sparse Core Ops, SparseCore 0:
  30.5 42.6 all-reduce.23
  88.8 55.2 all-reduce.17
  149.6 40.6 all-reduce.21
  206.2 55.2 all-reduce.19
where the time goes:
time: 270 us; the launch traced here: 269 us
  waiting for transfers between devices  188 us (70%)
  blocking collectives  33.7 us (12%)
  other arithmetic  16.8 us (6%)
  between operations  15.2 us (6%)
  matrix products  11.1 us (4%)
  local copies, waits for them, and re-layouts  3.91 us (1%)
    unnamed x7, waiting for transfers between devices  133 us
    psum x1, waiting for transfers between devices, body(): summed = lax.psum(partial_out, 'tp')  55.4 us
    all_gather x2, blocking collectives, body(): lax.all_gather(gated, 'dp', axis=0, tiled=True)  17.8 us
    all_gather x1, blocking collectives, body(): gathered = lax.all_gather(current, 'tp', axis=0, tiled=True)  15.9 us
  transfers between devices with their start and end apart: 4, of which 4 were waited for; matrix products, arithmetic and copies ran while one was open for 2% of the time, Pallas kernels for 0%

commit v1 on v0

--- a/solution.py
+++ b/solution.py
@@ -34,8 +34,49 @@
     return (readout.reshape(batch_size, -1), new_memory, new_normalizer, new_max)
 
 
+def peers(axis):
+    size = lax.axis_size(axis)
+    return size, lax.axis_index(axis)
+
+
+def gather_direct(rows, axis):
+    size, own = peers(axis)
+    pieces = [rows]
+    for step in range(1, size):
+        pieces.append(lax.ppermute(rows, axis, [(j, (j - step) % size) for j in range(size)]))
+    twice = jnp.stack(pieces + pieces)
+    ordered = lax.dynamic_slice_in_dim(twice, size - own, size, 0)
+    return ordered.reshape((size * rows.shape[0],) + rows.shape[1:])
+
+
+def scatter_direct(terms, axis):
+    size, own = peers(axis)
+    parts = terms.reshape((size, terms.shape[0] // size) + terms.shape[1:])
+    total = lax.dynamic_index_in_dim(parts, own, 0, keepdims=False).astype(jnp.float32)
+    received = []
+    for step in range(1, size):
+        part = lax.dynamic_index_in_dim(parts, (own + step) % size, 0, keepdims=False)
+        received.append(lax.ppermute(part, axis, [(j, (j + step) % size) for j in range(size)]))
+    for part in received:
+        total = total + part.astype(jnp.float32)
+    return total
+
+
+def sum_direct(term, axis):
+    size, _ = peers(axis)
+    sent = term.astype(jnp.bfloat16)
+    received = [
+        lax.ppermute(sent, axis, [(j, (j + step) % size) for j in range(size)])
+        for step in range(1, size)
+    ]
+    total = term
+    for part in received:
+        total = total + part.astype(jnp.float32)
+    return total
+
+
 def finish_split(partial_out, wide_rows):
-    summed = lax.psum_scatter(partial_out, "tp", scatter_dimension=0, tiled=True)
+    summed = scatter_direct(partial_out.astype(jnp.bfloat16), "tp")
     own_rows = lax.dynamic_slice_in_dim(
         wide_rows, lax.axis_index("tp") * summed.shape[0], summed.shape[0], 0
     )
@@ -57,10 +98,8 @@
     stabilizer,
 ):
     heads_here = w_query.shape[2] // HEAD_SIZE
-    seq_here = memory.shape[1]
     all_heads = w_gates.shape[2] // 2
     head_first = lax.axis_index("tp") * heads_here
-    seq_first = lax.axis_index("dp") * seq_here
     current = tokens
     gathered = None
     memories = []
@@ -68,7 +107,7 @@
     maxima = []
     for layer_index in range(2):
         if gathered is None:
-            gathered = lax.all_gather(current, "tp", axis=0, tiled=True)
+            gathered = gather_direct(current, "tp")
         wide_rows = gathered.astype(jnp.float32)
         square_part = jnp.sum(wide_rows * wide_rows, axis=1)
         scaled = (wide_rows * norm_gain[layer_index].astype(jnp.float32)[None, :]).astype(
@@ -87,15 +126,20 @@
         term_value = jnp.dot(scaled, w_value[layer_index], preferred_element_type=jnp.float32)
         term_outgate = jnp.dot(scaled, w_outgate[layer_index], preferred_element_type=jnp.float32)
         term_gates = jnp.dot(scaled, own_gates, preferred_element_type=jnp.float32)
-        square_all = lax.psum(square_part, "dp")
-        square_own = lax.dynamic_slice_in_dim(square_all, seq_first, seq_here, 0)
-        sum_query, sum_key, sum_value, sum_outgate, sum_gates = (
-            lax.psum_scatter(term_query, "dp", scatter_dimension=0, tiled=True),
-            lax.psum_scatter(term_key, "dp", scatter_dimension=0, tiled=True),
-            lax.psum_scatter(term_value, "dp", scatter_dimension=0, tiled=True),
-            lax.psum_scatter(term_outgate, "dp", scatter_dimension=0, tiled=True),
-            lax.psum_scatter(term_gates, "dp", scatter_dimension=0, tiled=True),
-        )
+        width = term_query.shape[1]
+        own = scatter_direct(
+            jnp.concatenate(
+                [term_query, term_key, term_value, term_outgate, term_gates, square_part[:, None]],
+                axis=1,
+            ),
+            "dp",
+        )
+        sum_query = own[:, :width]
+        sum_key = own[:, width : 2 * width]
+        sum_value = own[:, 2 * width : 3 * width]
+        sum_outgate = own[:, 3 * width : 4 * width]
+        sum_gates = own[:, 4 * width : 4 * width + 2 * heads_here]
+        square_own = own[:, 4 * width + 2 * heads_here]
         inv_scale = lax.rsqrt(square_own / D + epsilon)[:, None]
         query = (sum_query * inv_scale).astype(jnp.bfloat16)
         key_rows = (sum_key * inv_scale).astype(jnp.bfloat16)
@@ -118,12 +162,12 @@
         gated = (jax.nn.sigmoid(outgate.astype(jnp.float32)) * readout).astype(jnp.bfloat16)
         out_weight = w_out[layer_index]
         partial_out = jnp.dot(
-            lax.all_gather(gated, "dp", axis=0, tiled=True),
+            gather_direct(gated, "dp"),
             out_weight,
             preferred_element_type=jnp.float32,
         )
         if layer_index == 0:
-            summed = lax.psum(partial_out, "tp")
+            summed = sum_direct(partial_out, "tp")
             gathered = (wide_rows + summed).astype(jnp.bfloat16)
         else:
             current = finish_split(partial_out, wide_rows)

time: 270 us -> 88.5 us (0.33)
  waiting for transfers between devices: 188 us -> 21.6 us
  starting transfers between devices: 0.16 us -> 38.6 us
  blocking collectives: 33.7 us -> 0 us
  between operations: 15.2 us -> 1.16 us
  matrix products: 11.1 us -> 3.48 us
  local copies, waits for them, and re-layouts: 3.91 us -> 10.1 us
  other arithmetic: 16.8 us -> 12.9 us
    unnamed x7 -> x0, waiting for transfers between devices: 133 us -> none
    psum x1 -> x0, waiting for transfers between devices: 55.4 us -> none  [body(): summed = lax.psum(partial_out, 'tp')]
    ppermute x0 -> x33, starting transfers between devices: none -> 38.6 us  [the longest x13 17 us: gather_direct(): lax.ppermute(rows, axis, [(j, (j - step) % size) for j in range(size)])]
    all_gather x3 -> x0, blocking collectives: 33.7 us -> none  [the longest x2 17.8 us: body(): lax.all_gather(gated, 'dp', axis=0, tiled=True)]
    ppermute x0 -> x33, waiting for transfers between devices: none -> 21.6 us  [the longest x7 8.45 us: sum_direct(): lax.ppermute(sent, axis, [(j, (j + step) % size) for j in range(size)])]
    exp x0 -> x2, other arithmetic: none -> 3 us  [cell_update(): keep_factor = jnp.exp(carried - new_max)]
    unnamed x30 -> x61, local copies, waits for them, and re-layouts: 3.18 us -> 5.94 us
  transfers between devices with their start and end apart: 4 -> 33, of which waited for: 4 -> 12; matrix products, arithmetic and copies ran while one was open for 2% -> 9% of each run, Pallas kernels for 0% -> 0%
where the time goes in v1:
time: 88.5 us; the launch traced here: 87.9 us
  starting transfers between devices  38.6 us (44%)
  waiting for transfers between devices  21.6 us (24%)
  other arithmetic  12.9 us (15%)
  local copies, waits for them, and re-layouts  10.1 us (11%)
  matrix products  3.48 us (4%)
  between operations  1.16 us (1%)
    ppermute x13, starting transfers between devices, gather_direct(): lax.ppermute(rows, axis, [(j, (j - step) % size) for j in range(size)])  17 us
    ppermute x13, starting transfers between devices, scatter_direct(): lax.ppermute(part, axis, [(j, (j + step) % size) for j in range(size)])  16.8 us
    ppermute x7, waiting for transfers between devices, sum_direct(): lax.ppermute(sent, axis, [(j, (j + step) % size) for j in range(size)])  8.45 us
    ppermute x13, waiting for transfers between devices, gather_direct(): lax.ppermute(rows, axis, [(j, (j - step) % size) for j in range(size)])  7.1 us
    ppermute x13, waiting for transfers between devices, scatter_direct(): lax.ppermute(part, axis, [(j, (j + step) % size) for j in range(size)])  6.11 us
    unnamed x61, local copies, waits for them, and re-layouts  5.94 us
    ppermute x7, starting transfers between devices, sum_direct(): lax.ppermute(sent, axis, [(j, (j + step) % size) for j in range(size)])  4.79 us
    exp x2, other arithmetic, cell_update(): keep_factor = jnp.exp(carried - new_max)  3 us
  transfers between devices with their start and end apart: 33, of which 12 were waited for; matrix products, arithmetic and copies ran while one was open for 9% of the time, Pallas kernels for 0%

profile of v1, /device:TPU:0, one launch (start us, length us, event | category | flops | bytes accessed | tf_op | source)
XLA Modules:
  0.0 87.9 jit_solution(13860686503877278638)
XLA Ops:
  0.6 2.5 %collective-permute-start.4 = (bf16[4,1024]{1,0:T(4,128)(2,1)}, bf16[4,1024]{1,0:T(4,128)(2,1)S(1)}, u32[]{:S(2)}, u32[]{:S(2)}) collective-permute-start(bf16[4,1024]{1,0:T(4,128)(2,1)} %param.12), channel_id=1, source_target_pairs={{0,12},{4,16},{8,20},{12,24},{16,28},{20,0},{24,4},{28,8},{1,13},{... | collective-permute-start | bytes 24584 | tf_op jit(solution)/shard_map/ppermute | solution.py:46
  3.2 2.6 %collective-permute-start.3 = (bf16[4,1024]{1,0:T(4,128)(2,1)}, bf16[4,1024]{1,0:T(4,128)(2,1)S(1)}, u32[]{:S(2)}, u32[]{:S(2)}) collective-permute-start(bf16[4,1024]{1,0:T(4,128)(2,1)} %param.12), channel_id=1, source_target_pairs={{0,16},{4,20},{8,24},{12,28},{16,0},{20,4},{24,8},{28,12},{1,17},{... | collective-permute-start | bytes 24584 | tf_op jit(solution)/shard_map/ppermute | solution.py:46
  5.8 1.3 %collective-permute-start.2 = (bf16[4,1024]{1,0:T(4,128)(2,1)}, bf16[4,1024]{1,0:T(4,128)(2,1)S(1)}, u32[]{:S(2)}, u32[]{:S(2)}) collective-permute-start(bf16[4,1024]{1,0:T(4,128)(2,1)} %param.12), channel_id=1, source_target_pairs={{0,20},{4,24},{8,28},{12,0},{16,4},{20,8},{24,12},{28,16},{1,21},{... | collective-permute-start | bytes 24584 | tf_op jit(solution)/shard_map/ppermute | solution.py:46
  7.1 1.3 %collective-permute-start.1 = (bf16[4,1024]{1,0:T(4,128)(2,1)}, bf16[4,1024]{1,0:T(4,128)(2,1)S(1)}, u32[]{:S(2)}, u32[]{:S(2)}) collective-permute-start(bf16[4,1024]{1,0:T(4,128)(2,1)} %param.12), channel_id=1, source_target_pairs={{0,24},{4,28},{8,0},{12,4},{16,8},{20,12},{24,16},{28,20},{1,25},{... | collective-permute-start | bytes 24584 | tf_op jit(solution)/shard_map/ppermute | solution.py:46
  9.5 1.2 %slice_bitcast_fusion.3 = (f32[8,1]{0,1:T(1,128)S(1)}, f32[8,1]{0,1:T(1,128)}) fusion(f32[2,8,1]{1,2,0:T(1,128)} %param.23), kind=kLoop, calls=%fused_computation.205 | loop fusion | bytes 128 | tf_op jit(solution)/shard_map/squeeze | solution.py:160
  10.7 1.4 %slice_convert_fusion = (f32[1,1024]{1,0:T(1,128)}, f32[1,1024]{1,0:T(1,128)S(1)}) fusion(bf16[2,1024]{1,0:T(2,128)(2,1)} %param.13), kind=kLoop, calls=%fused_computation.186 | loop fusion | flops 2048 | bytes 12288 | tf_op jit(solution)/shard_map/mul | solution.py:113
  13.2 1.0 %collective-permute-start.5 = (bf16[4,1024]{1,0:T(4,128)(2,1)}, bf16[4,1024]{1,0:T(4,128)(2,1)S(1)}, u32[]{:S(2)}, u32[]{:S(2)}) collective-permute-start(bf16[4,1024]{1,0:T(4,128)(2,1)} %param.12), channel_id=1, source_target_pairs={{0,8},{4,12},{8,16},{12,20},{16,24},{20,28},{24,0},{28,4},{1,9},{5... | collective-permute-start | bytes 24584 | tf_op jit(solution)/shard_map/ppermute | solution.py:46
  14.3 4.6 %collective-permute-done.5 = bf16[4,1024]{1,0:T(4,128)(2,1)S(1)} collective-permute-done((bf16[4,1024]{1,0:T(4,128)(2,1)}, bf16[4,1024]{1,0:T(4,128)(2,1)S(1)}, u32[]{:S(2)}, u32[]{:S(2)}) %collective-permute-start.5) | collective-permute-done | bytes 8224 | tf_op jit(solution)/shard_map/ppermute | solution.py:46
  21.0 1.1 %fusion.23 = f32[4,8,128]{2,1,0:T(8,128)S(1)} fusion(bf16[4,8,1024]{2,1,0:T(8,128)(2,1)S(1)} %dot_general.40, bf16[2,1024,128]{2,1,0:T(8,128)(2,1)} %param.14), kind=kOutput, calls=%fused_computation.30 | convolution fusion | flops 8388608 | bytes 344064 | tf_op jit(solution)/shard_map/dot_general | solution.py:124
  22.4 1.5 %collective-permute-start.7 = (f32[8,515]{1,0:T(8,128)S(1)}, f32[8,515]{1,0:T(8,128)S(1)}, u32[]{:S(2)}, u32[]{:S(2)}) collective-permute-start(f32[8,515]{1,0:T(8,128)S(1)} %get-tuple-element.47), channel_id=1, source_target_pairs={{0,1},{1,2},{2,3},{3,0},{4,5},{5,6},{6,7},{7,4},{8,9},{9,10},{10,1... | collective-permute-start | bytes 49448 | tf_op jit(solution)/shard_map/ppermute | solution.py:59
  23.9 1.4 %collective-permute-start.9 = (f32[8,515]{1,0:T(8,128)S(1)}, f32[8,515]{1,0:T(8,128)S(1)}, u32[]{:S(2)}, u32[]{:S(2)}) collective-permute-start(f32[8,515]{1,0:T(8,128)S(1)} %get-tuple-element.48), channel_id=1, source_target_pairs={{0,3},{1,0},{2,1},{3,2},{4,7},{5,4},{6,5},{7,6},{8,11},{9,8},{10,9... | collective-permute-start | bytes 49448 | tf_op jit(solution)/shard_map/ppermute | solution.py:59
  25.4 1.5 %collective-permute-start.8 = (f32[8,515]{1,0:T(8,128)S(1)}, f32[8,515]{1,0:T(8,128)S(1)}, u32[]{:S(2)}, u32[]{:S(2)}) collective-permute-start(f32[8,515]{1,0:T(8,128)S(1)} %get-tuple-element.49), channel_id=1, source_target_pairs={{0,2},{1,3},{2,0},{3,1},{4,6},{5,7},{6,4},{7,5},{8,10},{9,11},{10,... | collective-permute-start | bytes 49448 | tf_op jit(solution)/shard_map/ppermute | solution.py:59
  27.7 1.4 %collective-permute-done.8 = f32[8,515]{1,0:T(8,128)S(1)} collective-permute-done((f32[8,515]{1,0:T(8,128)S(1)}, f32[8,515]{1,0:T(8,128)S(1)}, u32[]{:S(2)}, u32[]{:S(2)}) %collective-permute-start.8) | collective-permute-done | bytes 16512 | tf_op jit(solution)/shard_map/ppermute | solution.py:59
  29.4 1.5 %exponential_reduce_fusion.3 = (f32[8]{0:T(128)S(1)}, f32[8]{0:T(128)S(1)}, f32[8,1]{1,0:T(8,128)S(1)}) fusion(f32[8,1]{1,0:T(8,128)S(1)} %copy.46, f32[]{:T(128)} %bitcast.24, f32[8,2]{1,0:T(8,128)S(1)} %slice_multiply_fusion.9, f32[]{:T(128)} %bitcast.26), kind=kLoop, calls=%fused_computation.192 | loop fusion | flops 112 | bytes 200 | tf_op jit(solution)/shard_map/exp | solution.py:23
  33.1 1.6 %collective-permute-start.10 = (bf16[8,128]{1,0:T(8,128)(2,1)S(1)}, bf16[8,128]{1,0:T(8,128)(2,1)S(1)}, u32[]{:S(2)}, u32[]{:S(2)}) collective-permute-start(bf16[8,128]{1,0:T(8,128)(2,1)S(1)} %get-tuple-element.36), channel_id=1, source_target_pairs={{0,3},{1,0},{2,1},{3,2},{4,7},{5,4},{6,5},{7,6},{8,11},{9,8},{10,9... | collective-permute-start | bytes 6152 | tf_op jit(solution)/shard_map/ppermute | solution.py:46
  35.1 1.5 %collective-permute-start.11 = (bf16[8,128]{1,0:T(8,128)(2,1)S(1)}, bf16[8,128]{1,0:T(8,128)(2,1)S(1)}, u32[]{:S(2)}, u32[]{:S(2)}) collective-permute-start(bf16[8,128]{1,0:T(8,128)(2,1)S(1)} %get-tuple-element.36), channel_id=1, source_target_pairs={{0,2},{1,3},{2,0},{3,1},{4,6},{5,7},{6,4},{7,5},{8,10},{9,11},{10,... | collective-permute-start | bytes 6152 | tf_op jit(solution)/shard_map/ppermute | solution.py:46
  36.7 2.0 %collective-permute-done.11 = bf16[8,128]{1,0:T(8,128)(2,1)S(1)} collective-permute-done((bf16[8,128]{1,0:T(8,128)(2,1)S(1)}, bf16[8,128]{1,0:T(8,128)(2,1)S(1)}, u32[]{:S(2)}, u32[]{:S(2)}) %collective-permute-start.11) | collective-permute-done | bytes 2080 | tf_op jit(solution)/shard_map/ppermute | solution.py:46
  40.5 2.5 %collective-permute-start.16 = (bf16[32,1024]{1,0:T(8,128)(2,1)}, bf16[32,1024]{1,0:T(8,128)(2,1)}, u32[]{:S(2)}, u32[]{:S(2)}) collective-permute-start(bf16[32,1024]{1,0:T(8,128)(2,1)} %get-tuple-element.75), channel_id=1, source_target_pairs={{0,16},{4,20},{8,24},{12,28},{16,0},{20,4},{24,8},{28,12},{1,17},{... | collective-permute-start | bytes 196616 | tf_op jit(solution)/shard_map/ppermute | solution.py:69
  43.1 1.7 %collective-permute-start.14 = (bf16[32,1024]{1,0:T(8,128)(2,1)}, bf16[32,1024]{1,0:T(8,128)(2,1)}, u32[]{:S(2)}, u32[]{:S(2)}) collective-permute-start(bf16[32,1024]{1,0:T(8,128)(2,1)} %get-tuple-element.75), channel_id=1, source_target_pairs={{0,8},{4,12},{8,16},{12,20},{16,24},{20,28},{24,0},{28,4},{1,9},{5... | collective-permute-start | bytes 196616 | tf_op jit(solution)/shard_map/ppermute | solution.py:69
  46.3 7.0 %collective-permute-done.16 = bf16[32,1024]{1,0:T(8,128)(2,1)} collective-permute-done((bf16[32,1024]{1,0:T(8,128)(2,1)}, bf16[32,1024]{1,0:T(8,128)(2,1)}, u32[]{:S(2)}, u32[]{:S(2)}) %collective-permute-start.16) | collective-permute-done | bytes 65568 | tf_op jit(solution)/shard_map/ppermute | solution.py:69
  53.9 1.7 %multiply_reduce_fusion = (f32[32]{0:T(128)}, f32[32,1024]{1,0:T(8,128)S(1)}) fusion(f32[32,1024]{1,0:T(8,128)S(1)} %reshape.279, bf16[32,1024]{1,0:T(8,128)(2,1)} %collective-permute-done.19, bf16[32,1024]{1,0:T(8,128)(2,1)} %collective-permute-done.18, bf16[32,1024]{1,0:T(8,128)(2,1)} %collective-permute-done.17, ...), kind=kLoop, calls=%fused_computation.42 | loop fusion | flops 622560 | bytes 852096 | tf_op jit(solution)/shard_map/reduce_sum | solution.py:112
  59.1 1.5 %collective-permute-start.20 = (f32[8,515]{1,0:T(8,128)S(1)}, f32[8,515]{1,0:T(8,128)S(1)}, u32[]{:S(2)}, u32[]{:S(2)}) collective-permute-start(f32[8,515]{1,0:T(8,128)S(1)} %get-tuple-element.44), channel_id=1, source_target_pairs={{0,1},{1,2},{2,3},{3,0},{4,5},{5,6},{6,7},{7,4},{8,9},{9,10},{10,1... | collective-permute-start | bytes 49448 | tf_op jit(solution)/shard_map/ppermute | solution.py:59
  60.7 1.5 %collective-permute-start.22 = (f32[8,515]{1,0:T(8,128)S(1)}, f32[8,515]{1,0:T(8,128)S(1)}, u32[]{:S(2)}, u32[]{:S(2)}) collective-permute-start(f32[8,515]{1,0:T(8,128)S(1)} %get-tuple-element.45), channel_id=1, source_target_pairs={{0,3},{1,0},{2,1},{3,2},{4,7},{5,4},{6,5},{7,6},{8,11},{9,8},{10,9... | collective-permute-start | bytes 49448 | tf_op jit(solution)/shard_map/ppermute | solution.py:59
  62.1 1.1 %collective-permute-start.21 = (f32[8,515]{1,0:T(8,128)S(1)}, f32[8,515]{1,0:T(8,128)S(1)}, u32[]{:S(2)}, u32[]{:S(2)}) collective-permute-start(f32[8,515]{1,0:T(8,128)S(1)} %get-tuple-element.46), channel_id=1, source_target_pairs={{0,2},{1,3},{2,0},{3,1},{4,6},{5,7},{6,4},{7,5},{8,10},{9,11},{10,... | collective-permute-start | bytes 49448 | tf_op jit(solution)/shard_map/ppermute | solution.py:59
  64.4 1.5 %collective-permute-done.21 = f32[8,515]{1,0:T(8,128)S(1)} collective-permute-done((f32[8,515]{1,0:T(8,128)S(1)}, f32[8,515]{1,0:T(8,128)S(1)}, u32[]{:S(2)}, u32[]{:S(2)}) %collective-permute-start.21) | collective-permute-done | bytes 16512 | tf_op jit(solution)/shard_map/ppermute | solution.py:59
  66.2 1.5 %exponential_reduce_fusion.1 = (f32[8]{0:T(128)S(1)}, f32[8]{0:T(128)S(1)}, f32[8,1]{1,0:T(8,128)S(1)}) fusion(f32[8,1]{1,0:T(8,128)S(1)} %copy.51, f32[]{:T(128)} %bitcast.54, f32[8,2]{1,0:T(8,128)S(1)} %slice_multiply_fusion.3, f32[]{:T(128)} %bitcast.56), kind=kLoop, calls=%fused_computation.184 | loop fusion | flops 112 | bytes 200 | tf_op jit(solution)/shard_map/exp | solution.py:23
  70.4 2.3 %collective-permute-start.23 = (bf16[8,128]{1,0:T(8,128)(2,1)S(1)}, bf16[8,128]{1,0:T(8,128)(2,1)S(1)}, u32[]{:S(2)}, u32[]{:S(2)}) collective-permute-start(bf16[8,128]{1,0:T(8,128)(2,1)S(1)} %get-tuple-element.29), channel_id=1, source_target_pairs={{0,3},{1,0},{2,1},{3,2},{4,7},{5,4},{6,5},{7,6},{8,11},{9,8},{10,9... | collective-permute-start | bytes 6152 | tf_op jit(solution)/shard_map/ppermute | solution.py:46
  73.2 1.0 %pad_maximum_fusion = f32[2,8,1,128,128]{4,3,2,1,0:T(8,128)} fusion(f32[1,8,1,128,128]{4,3,2,1,0:T(8,128)S(1)} %get-tuple-element.41, f32[1,8,1,128,128]{4,3,2,1,0:T(8,128)S(1)} %get-tuple-element.40), kind=kLoop, calls=%fused_computation.2 | loop fusion | flops 262144 | bytes 2097152 | tf_op jit(solution)/shard_map/stack | solution.py:177
  74.6 3.5 %collective-permute-start.32 = (bf16[4,1024]{1,0:T(4,128)(2,1)S(1)}, bf16[4,1024]{1,0:T(4,128)(2,1)S(1)}, u32[]{:S(2)}, u32[]{:S(2)}) collective-permute-start(bf16[4,1024]{1,0:T(4,128)(2,1)S(1)} %get-tuple-element.51), channel_id=1, source_target_pairs={{0,28},{4,0},{8,4},{12,8},{16,12},{20,16},{24,20},{28,24},{1,29},{... | collective-permute-start | bytes 24584 | tf_op jit(solution)/shard_map/ppermute | solution.py:59
  78.8 2.6 %collective-permute-start.29 = (bf16[4,1024]{1,0:T(4,128)(2,1)S(1)}, bf16[4,1024]{1,0:T(4,128)(2,1)S(1)}, u32[]{:S(2)}, u32[]{:S(2)}) collective-permute-start(bf16[4,1024]{1,0:T(4,128)(2,1)S(1)} %get-tuple-element.54), channel_id=1, source_target_pairs={{0,16},{4,20},{8,24},{12,28},{16,0},{20,4},{24,8},{28,12},{1,17},{... | collective-permute-start | bytes 24584 | tf_op jit(solution)/shard_map/ppermute | solution.py:59
  81.4 1.9 %collective-permute-start.27 = (bf16[4,1024]{1,0:T(4,128)(2,1)S(1)}, bf16[4,1024]{1,0:T(4,128)(2,1)S(1)}, u32[]{:S(2)}, u32[]{:S(2)}) collective-permute-start(bf16[4,1024]{1,0:T(4,128)(2,1)S(1)} %get-tuple-element.56), channel_id=1, source_target_pairs={{0,8},{4,12},{8,16},{12,20},{16,24},{20,28},{24,0},{28,4},{1,9},{5... | collective-permute-start | bytes 24584 | tf_op jit(solution)/shard_map/ppermute | solution.py:59
  85.4 1.8 %collective-permute-done.27 = bf16[4,1024]{1,0:T(4,128)(2,1)S(1)} collective-permute-done((bf16[4,1024]{1,0:T(4,128)(2,1)S(1)}, bf16[4,1024]{1,0:T(4,128)(2,1)S(1)}, u32[]{:S(2)}, u32[]{:S(2)}) %collective-permute-start.27) | collective-permute-done | bytes 8224 | tf_op jit(solution)/shard_map/ppermute | solution.py:59
  (162 shorter events, 23.7 us)
Async XLA Ops:
  0.6 13.6 %collective-permute-start.4 = (bf16[4,1024]{1,0:T(4,128)(2,1)}, bf16[4,1024]{1,0:T(4,128)(2,1)S(1)}, u32[]{:S(2)}, u32[]{:S(2)}) collective-permute-start(bf16[4,1024]{1,0:T(4,128)(2,1)} %param.12), channel_id=1, source_target_pairs={{0,12},{4,16},{8,20},{12,24},{16,28},{20,0},{24,4},{28,8},{1,13},{... | collective-permute-start | bytes 24584 | tf_op jit(solution)/shard_map/ppermute | solution.py:46
  3.2 11.0 %collective-permute-start.3 = (bf16[4,1024]{1,0:T(4,128)(2,1)}, bf16[4,1024]{1,0:T(4,128)(2,1)S(1)}, u32[]{:S(2)}, u32[]{:S(2)}) collective-permute-start(bf16[4,1024]{1,0:T(4,128)(2,1)} %param.12), channel_id=1, source_target_pairs={{0,16},{4,20},{8,24},{12,28},{16,0},{20,4},{24,8},{28,12},{1,17},{... | collective-permute-start | bytes 24584 | tf_op jit(solution)/shard_map/ppermute | solution.py:46
  5.8 8.4 %collective-permute-start.2 = (bf16[4,1024]{1,0:T(4,128)(2,1)}, bf16[4,1024]{1,0:T(4,128)(2,1)S(1)}, u32[]{:S(2)}, u32[]{:S(2)}) collective-permute-start(bf16[4,1024]{1,0:T(4,128)(2,1)} %param.12), channel_id=1, source_target_pairs={{0,20},{4,24},{8,28},{12,0},{16,4},{20,8},{24,12},{28,16},{1,21},{... | collective-permute-start | bytes 24584 | tf_op jit(solution)/shard_map/ppermute | solution.py:46
  7.1 6.0 %collective-permute-start.1 = (bf16[4,1024]{1,0:T(4,128)(2,1)}, bf16[4,1024]{1,0:T(4,128)(2,1)S(1)}, u32[]{:S(2)}, u32[]{:S(2)}) collective-permute-start(bf16[4,1024]{1,0:T(4,128)(2,1)} %param.12), channel_id=1, source_target_pairs={{0,24},{4,28},{8,0},{12,4},{16,8},{20,12},{24,16},{28,20},{1,25},{... | collective-permute-start | bytes 24584 | tf_op jit(solution)/shard_map/ppermute | solution.py:46
  8.5 4.4 %collective-permute-start = (bf16[4,1024]{1,0:T(4,128)(2,1)}, bf16[4,1024]{1,0:T(4,128)(2,1)S(1)}, u32[]{:S(2)}, u32[]{:S(2)}) collective-permute-start(bf16[4,1024]{1,0:T(4,128)(2,1)} %param.12), channel_id=1, source_target_pairs={{0,28},{4,0},{8,4},{12,8},{16,12},{20,16},{24,20},{28,24},{1,29},{... | collective-permute-start | bytes 24584 | tf_op jit(solution)/shard_map/ppermute | solution.py:46
  12.9 6.0 %collective-permute-start.6 = (bf16[4,1024]{1,0:T(4,128)(2,1)}, bf16[4,1024]{1,0:T(4,128)(2,1)S(1)}, u32[]{:S(2)}, u32[]{:S(2)}) collective-permute-start(bf16[4,1024]{1,0:T(4,128)(2,1)} %param.12), channel_id=1, source_target_pairs={{0,4},{4,8},{8,12},{12,16},{16,20},{20,24},{24,28},{28,0},{1,5},{5... | collective-permute-start | bytes 24584 | tf_op jit(solution)/shard_map/ppermute | solution.py:46
  13.2 5.7 %collective-permute-start.5 = (bf16[4,1024]{1,0:T(4,128)(2,1)}, bf16[4,1024]{1,0:T(4,128)(2,1)S(1)}, u32[]{:S(2)}, u32[]{:S(2)}) collective-permute-start(bf16[4,1024]{1,0:T(4,128)(2,1)} %param.12), channel_id=1, source_target_pairs={{0,8},{4,12},{8,16},{12,20},{16,24},{20,28},{24,0},{28,4},{1,9},{5... | collective-permute-start | bytes 24584 | tf_op jit(solution)/shard_map/ppermute | solution.py:46
  22.4 5.2 %collective-permute-start.7 = (f32[8,515]{1,0:T(8,128)S(1)}, f32[8,515]{1,0:T(8,128)S(1)}, u32[]{:S(2)}, u32[]{:S(2)}) collective-permute-start(f32[8,515]{1,0:T(8,128)S(1)} %get-tuple-element.47), channel_id=1, source_target_pairs={{0,1},{1,2},{2,3},{3,0},{4,5},{5,6},{6,7},{7,4},{8,9},{9,10},{10,1... | collective-permute-start | bytes 49448 | tf_op jit(solution)/shard_map/ppermute | solution.py:59
  23.9 3.8 %collective-permute-start.9 = (f32[8,515]{1,0:T(8,128)S(1)}, f32[8,515]{1,0:T(8,128)S(1)}, u32[]{:S(2)}, u32[]{:S(2)}) collective-permute-start(f32[8,515]{1,0:T(8,128)S(1)} %get-tuple-element.48), channel_id=1, source_target_pairs={{0,3},{1,0},{2,1},{3,2},{4,7},{5,4},{6,5},{7,6},{8,11},{9,8},{10,9... | collective-permute-start | bytes 49448 | tf_op jit(solution)/shard_map/ppermute | solution.py:59
  25.4 3.8 %collective-permute-start.8 = (f32[8,515]{1,0:T(8,128)S(1)}, f32[8,515]{1,0:T(8,128)S(1)}, u32[]{:S(2)}, u32[]{:S(2)}) collective-permute-start(f32[8,515]{1,0:T(8,128)S(1)} %get-tuple-element.49), channel_id=1, source_target_pairs={{0,2},{1,3},{2,0},{3,1},{4,6},{5,7},{6,4},{7,5},{8,10},{9,11},{10,... | collective-permute-start | bytes 49448 | tf_op jit(solution)/shard_map/ppermute | solution.py:59
  33.1 3.6 %collective-permute-start.10 = (bf16[8,128]{1,0:T(8,128)(2,1)S(1)}, bf16[8,128]{1,0:T(8,128)(2,1)S(1)}, u32[]{:S(2)}, u32[]{:S(2)}) collective-permute-start(bf16[8,128]{1,0:T(8,128)(2,1)S(1)} %get-tuple-element.36), channel_id=1, source_target_pairs={{0,3},{1,0},{2,1},{3,2},{4,7},{5,4},{6,5},{7,6},{8,11},{9,8},{10,9... | collective-permute-start | bytes 6152 | tf_op jit(solution)/shard_map/ppermute | solution.py:46
  34.7 4.5 %collective-permute-start.12 = (bf16[8,128]{1,0:T(8,128)(2,1)S(1)}, bf16[8,128]{1,0:T(8,128)(2,1)S(1)}, u32[]{:S(2)}, u32[]{:S(2)}) collective-permute-start(bf16[8,128]{1,0:T(8,128)(2,1)S(1)} %get-tuple-element.36), channel_id=1, source_target_pairs={{0,1},{1,2},{2,3},{3,0},{4,5},{5,6},{6,7},{7,4},{8,9},{9,10},{10,1... | collective-permute-start | bytes 6152 | tf_op jit(solution)/shard_map/ppermute | solution.py:46
  35.1 3.6 %collective-permute-start.11 = (bf16[8,128]{1,0:T(8,128)(2,1)S(1)}, bf16[8,128]{1,0:T(8,128)(2,1)S(1)}, u32[]{:S(2)}, u32[]{:S(2)}) collective-permute-start(bf16[8,128]{1,0:T(8,128)(2,1)S(1)} %get-tuple-element.36), channel_id=1, source_target_pairs={{0,2},{1,3},{2,0},{3,1},{4,6},{5,7},{6,4},{7,5},{8,10},{9,11},{10,... | collective-permute-start | bytes 6152 | tf_op jit(solution)/shard_map/ppermute | solution.py:46
  40.0 5.6 %collective-permute-start.18 = (bf16[32,1024]{1,0:T(8,128)(2,1)}, bf16[32,1024]{1,0:T(8,128)(2,1)}, u32[]{:S(2)}, u32[]{:S(2)}) collective-permute-start(bf16[32,1024]{1,0:T(8,128)(2,1)} %get-tuple-element.75), channel_id=1, source_target_pairs={{0,24},{4,28},{8,0},{12,4},{16,8},{20,12},{24,16},{28,20},{1,25},{... | collective-permute-start | bytes 196616 | tf_op jit(solution)/shard_map/ppermute | solution.py:69
  40.0 6.3 %collective-permute-start.17 = (bf16[32,1024]{1,0:T(8,128)(2,1)}, bf16[32,1024]{1,0:T(8,128)(2,1)}, u32[]{:S(2)}, u32[]{:S(2)}) collective-permute-start(bf16[32,1024]{1,0:T(8,128)(2,1)} %get-tuple-element.75), channel_id=1, source_target_pairs={{0,20},{4,24},{8,28},{12,0},{16,4},{20,8},{24,12},{28,16},{1,21},{... | collective-permute-start | bytes 196616 | tf_op jit(solution)/shard_map/ppermute | solution.py:69
  40.5 12.8 %collective-permute-start.16 = (bf16[32,1024]{1,0:T(8,128)(2,1)}, bf16[32,1024]{1,0:T(8,128)(2,1)}, u32[]{:S(2)}, u32[]{:S(2)}) collective-permute-start(bf16[32,1024]{1,0:T(8,128)(2,1)} %get-tuple-element.75), channel_id=1, source_target_pairs={{0,16},{4,20},{8,24},{12,28},{16,0},{20,4},{24,8},{28,12},{1,17},{... | collective-permute-start | bytes 196616 | tf_op jit(solution)/shard_map/ppermute | solution.py:69
  43.0 10.9 %collective-permute-start.15 = (bf16[32,1024]{1,0:T(8,128)(2,1)}, bf16[32,1024]{1,0:T(8,128)(2,1)}, u32[]{:S(2)}, u32[]{:S(2)}) collective-permute-start(bf16[32,1024]{1,0:T(8,128)(2,1)} %get-tuple-element.75), channel_id=1, source_target_pairs={{0,12},{4,16},{8,20},{12,24},{16,28},{20,0},{24,4},{28,8},{1,13},{... | collective-permute-start | bytes 196616 | tf_op jit(solution)/shard_map/ppermute | solution.py:69
  43.1 10.9 %collective-permute-start.14 = (bf16[32,1024]{1,0:T(8,128)(2,1)}, bf16[32,1024]{1,0:T(8,128)(2,1)}, u32[]{:S(2)}, u32[]{:S(2)}) collective-permute-start(bf16[32,1024]{1,0:T(8,128)(2,1)} %get-tuple-element.75), channel_id=1, source_target_pairs={{0,8},{4,12},{8,16},{12,20},{16,24},{20,28},{24,0},{28,4},{1,9},{5... | collective-permute-start | bytes 196616 | tf_op jit(solution)/shard_map/ppermute | solution.py:69
  45.6 8.3 %collective-permute-start.13 = (bf16[32,1024]{1,0:T(8,128)(2,1)}, bf16[32,1024]{1,0:T(8,128)(2,1)}, u32[]{:S(2)}, u32[]{:S(2)}) collective-permute-start(bf16[32,1024]{1,0:T(8,128)(2,1)} %get-tuple-element.75), channel_id=1, source_target_pairs={{0,4},{4,8},{8,12},{12,16},{16,20},{20,24},{24,28},{28,0},{1,5},{5... | collective-permute-start | bytes 196616 | tf_op jit(solution)/shard_map/ppermute | solution.py:69
  59.1 4.8 %collective-permute-start.20 = (f32[8,515]{1,0:T(8,128)S(1)}, f32[8,515]{1,0:T(8,128)S(1)}, u32[]{:S(2)}, u32[]{:S(2)}) collective-permute-start(f32[8,515]{1,0:T(8,128)S(1)} %get-tuple-element.44), channel_id=1, source_target_pairs={{0,1},{1,2},{2,3},{3,0},{4,5},{5,6},{6,7},{7,4},{8,9},{9,10},{10,1... | collective-permute-start | bytes 49448 | tf_op jit(solution)/shard_map/ppermute | solution.py:59
  60.7 3.8 %collective-permute-start.22 = (f32[8,515]{1,0:T(8,128)S(1)}, f32[8,515]{1,0:T(8,128)S(1)}, u32[]{:S(2)}, u32[]{:S(2)}) collective-permute-start(f32[8,515]{1,0:T(8,128)S(1)} %get-tuple-element.45), channel_id=1, source_target_pairs={{0,3},{1,0},{2,1},{3,2},{4,7},{5,4},{6,5},{7,6},{8,11},{9,8},{10,9... | collective-permute-start | bytes 49448 | tf_op jit(solution)/shard_map/ppermute | solution.py:59
  62.1 3.8 %collective-permute-start.21 = (f32[8,515]{1,0:T(8,128)S(1)}, f32[8,515]{1,0:T(8,128)S(1)}, u32[]{:S(2)}, u32[]{:S(2)}) collective-permute-start(f32[8,515]{1,0:T(8,128)S(1)} %get-tuple-element.46), channel_id=1, source_target_pairs={{0,2},{1,3},{2,0},{3,1},{4,6},{5,7},{6,4},{7,5},{8,10},{9,11},{10,... | collective-permute-start | bytes 49448 | tf_op jit(solution)/shard_map/ppermute | solution.py:59
  68.7 5.6 %collective-permute-start.25 = (bf16[8,128]{1,0:T(8,128)(2,1)S(1)}, bf16[8,128]{1,0:T(8,128)(2,1)S(1)}, u32[]{:S(2)}, u32[]{:S(2)}) collective-permute-start(bf16[8,128]{1,0:T(8,128)(2,1)S(1)} %get-tuple-element.29), channel_id=1, source_target_pairs={{0,1},{1,2},{2,3},{3,0},{4,5},{5,6},{6,7},{7,4},{8,9},{9,10},{10,1... | collective-permute-start | bytes 6152 | tf_op jit(solution)/shard_map/ppermute | solution.py:46
  69.5 4.7 %collective-permute-start.24 = (bf16[8,128]{1,0:T(8,128)(2,1)S(1)}, bf16[8,128]{1,0:T(8,128)(2,1)S(1)}, u32[]{:S(2)}, u32[]{:S(2)}) collective-permute-start(bf16[8,128]{1,0:T(8,128)(2,1)S(1)} %get-tuple-element.29), channel_id=1, source_target_pairs={{0,2},{1,3},{2,0},{3,1},{4,6},{5,7},{6,4},{7,5},{8,10},{9,11},{10,... | collective-permute-start | bytes 6152 | tf_op jit(solution)/shard_map/ppermute | solution.py:46
  70.4 3.8 %collective-permute-start.23 = (bf16[8,128]{1,0:T(8,128)(2,1)S(1)}, bf16[8,128]{1,0:T(8,128)(2,1)S(1)}, u32[]{:S(2)}, u32[]{:S(2)}) collective-permute-start(bf16[8,128]{1,0:T(8,128)(2,1)S(1)} %get-tuple-element.29), channel_id=1, source_target_pairs={{0,3},{1,0},{2,1},{3,2},{4,7},{5,4},{6,5},{7,6},{8,11},{9,8},{10,9... | collective-permute-start | bytes 6152 | tf_op jit(solution)/shard_map/ppermute | solution.py:46
  74.6 6.9 %collective-permute-start.26 = (bf16[4,1024]{1,0:T(4,128)(2,1)S(1)}, bf16[4,1024]{1,0:T(4,128)(2,1)S(1)}, u32[]{:S(2)}, u32[]{:S(2)}) collective-permute-start(bf16[4,1024]{1,0:T(4,128)(2,1)S(1)} %get-tuple-element.50), channel_id=1, source_target_pairs={{0,4},{4,8},{8,12},{12,16},{16,20},{20,24},{24,28},{28,0},{1,5},{5... | collective-permute-start | bytes 24584 | tf_op jit(solution)/shard_map/ppermute | solution.py:59
  74.6 6.8 %collective-permute-start.32 = (bf16[4,1024]{1,0:T(4,128)(2,1)S(1)}, bf16[4,1024]{1,0:T(4,128)(2,1)S(1)}, u32[]{:S(2)}, u32[]{:S(2)}) collective-permute-start(bf16[4,1024]{1,0:T(4,128)(2,1)S(1)} %get-tuple-element.51), channel_id=1, source_target_pairs={{0,28},{4,0},{8,4},{12,8},{16,12},{20,16},{24,20},{28,24},{1,29},{... | collective-permute-start | bytes 24584 | tf_op jit(solution)/shard_map/ppermute | solution.py:59
  78.8 5.8 %collective-permute-start.31 = (bf16[4,1024]{1,0:T(4,128)(2,1)S(1)}, bf16[4,1024]{1,0:T(4,128)(2,1)S(1)}, u32[]{:S(2)}, u32[]{:S(2)}) collective-permute-start(bf16[4,1024]{1,0:T(4,128)(2,1)S(1)} %get-tuple-element.52), channel_id=1, source_target_pairs={{0,24},{4,28},{8,0},{12,4},{16,8},{20,12},{24,16},{28,20},{1,25},{... | collective-permute-start | bytes 24584 | tf_op jit(solution)/shard_map/ppermute | solution.py:59
  78.8 5.8 %collective-permute-start.30 = (bf16[4,1024]{1,0:T(4,128)(2,1)S(1)}, bf16[4,1024]{1,0:T(4,128)(2,1)S(1)}, u32[]{:S(2)}, u32[]{:S(2)}) collective-permute-start(bf16[4,1024]{1,0:T(4,128)(2,1)S(1)} %get-tuple-element.53), channel_id=1, source_target_pairs={{0,20},{4,24},{8,28},{12,0},{16,4},{20,8},{24,12},{28,16},{1,21},{... | collective-permute-start | bytes 24584 | tf_op jit(solution)/shard_map/ppermute | solution.py:59
  78.8 5.8 %collective-permute-start.29 = (bf16[4,1024]{1,0:T(4,128)(2,1)S(1)}, bf16[4,1024]{1,0:T(4,128)(2,1)S(1)}, u32[]{:S(2)}, u32[]{:S(2)}) collective-permute-start(bf16[4,1024]{1,0:T(4,128)(2,1)S(1)} %get-tuple-element.54), channel_id=1, source_target_pairs={{0,16},{4,20},{8,24},{12,28},{16,0},{20,4},{24,8},{28,12},{1,17},{... | collective-permute-start | bytes 24584 | tf_op jit(solution)/shard_map/ppermute | solution.py:59
  81.4 4.0 %collective-permute-start.28 = (bf16[4,1024]{1,0:T(4,128)(2,1)S(1)}, bf16[4,1024]{1,0:T(4,128)(2,1)S(1)}, u32[]{:S(2)}, u32[]{:S(2)}) collective-permute-start(bf16[4,1024]{1,0:T(4,128)(2,1)S(1)} %get-tuple-element.55), channel_id=1, source_target_pairs={{0,12},{4,16},{8,20},{12,24},{16,28},{20,0},{24,4},{28,8},{1,13},{... | collective-permute-start | bytes 24584 | tf_op jit(solution)/shard_map/ppermute | solution.py:59
  81.4 5.8 %collective-permute-start.27 = (bf16[4,1024]{1,0:T(4,128)(2,1)S(1)}, bf16[4,1024]{1,0:T(4,128)(2,1)S(1)}, u32[]{:S(2)}, u32[]{:S(2)}) collective-permute-start(bf16[4,1024]{1,0:T(4,128)(2,1)S(1)} %get-tuple-element.56), channel_id=1, source_target_pairs={{0,8},{4,12},{8,16},{12,20},{16,24},{20,28},{24,0},{28,4},{1,9},{5... | collective-permute-start | bytes 24584 | tf_op jit(solution)/shard_map/ppermute | solution.py:59
  (18 other events, 86.5 us)

commit v2 on v1

--- a/solution.py
+++ b/solution.py
@@ -62,21 +62,69 @@
     return total
 
 
-def sum_direct(term, axis):
-    size, _ = peers(axis)
-    sent = term.astype(jnp.bfloat16)
+def pairing(axis):
+    size, own = peers(axis)
+    inner = 2 if size % 2 == 0 else 1
+    return size, inner, size // inner, own // inner, own % inner
+
+
+def swap(value, axis, size):
+    return lax.ppermute(value, axis, [(j, j ^ 1) for j in range(size)])
+
+
+def gather_paired(rows, axis):
+    size, inner, groups, group, place = pairing(axis)
+    both = rows
+    if inner == 2:
+        other = swap(rows, axis, size)
+        both = jnp.concatenate(
+            [jnp.where(place == 0, rows, other), jnp.where(place == 0, other, rows)], axis=0
+        )
+    pieces = [both]
+    for step in range(1, groups):
+        hop = step * inner
+        pieces.append(lax.ppermute(both, axis, [(j, (j - hop) % size) for j in range(size)]))
+    twice = jnp.stack(pieces + pieces)
+    ordered = lax.dynamic_slice_in_dim(twice, groups - group, groups, 0)
+    return ordered.reshape((size * rows.shape[0],) + rows.shape[1:])
+
+
+def sum_paired(term, axis):
+    size, inner, groups, _, _ = pairing(axis)
+    total = term
+    if inner == 2:
+        total = total + swap(term.astype(jnp.bfloat16), axis, size).astype(jnp.float32)
+    sent = total.astype(jnp.bfloat16)
     received = [
-        lax.ppermute(sent, axis, [(j, (j + step) % size) for j in range(size)])
-        for step in range(1, size)
+        lax.ppermute(sent, axis, [(j, (j + step * inner) % size) for j in range(size)])
+        for step in range(1, groups)
     ]
-    total = term
     for part in received:
         total = total + part.astype(jnp.float32)
     return total
 
 
+def scatter_paired(term, axis):
+    size, inner, groups, group, place = pairing(axis)
+    parts = term.reshape((groups, inner, term.shape[0] // size) + term.shape[1:])
+    half = lax.dynamic_index_in_dim(parts, place, 1, keepdims=False)
+    if inner == 2:
+        given = lax.dynamic_index_in_dim(parts, 1 - place, 1, keepdims=False)
+        half = half + swap(given.astype(jnp.bfloat16), axis, size).astype(jnp.float32)
+    total = lax.dynamic_index_in_dim(half, group, 0, keepdims=False)
+    sent = half.astype(jnp.bfloat16)
+    received = []
+    for step in range(1, groups):
+        part = lax.dynamic_index_in_dim(sent, (group + step) % groups, 0, keepdims=False)
+        hop = step * inner
+        received.append(lax.ppermute(part, axis, [(j, (j + hop) % size) for j in range(size)]))
+    for part in received:
+        total = total + part.astype(jnp.float32)
+    return total
+
+
 def finish_split(partial_out, wide_rows):
-    summed = scatter_direct(partial_out.astype(jnp.bfloat16), "tp")
+    summed = scatter_paired(partial_out, "tp")
     own_rows = lax.dynamic_slice_in_dim(
         wide_rows, lax.axis_index("tp") * summed.shape[0], summed.shape[0], 0
     )
@@ -107,7 +155,7 @@
     maxima = []
     for layer_index in range(2):
         if gathered is None:
-            gathered = gather_direct(current, "tp")
+            gathered = gather_paired(current, "tp")
         wide_rows = gathered.astype(jnp.float32)
         square_part = jnp.sum(wide_rows * wide_rows, axis=1)
         scaled = (wide_rows * norm_gain[layer_index].astype(jnp.float32)[None, :]).astype(
@@ -167,7 +215,7 @@
             preferred_element_type=jnp.float32,
         )
         if layer_index == 0:
-            summed = sum_direct(partial_out, "tp")
+            summed = sum_paired(partial_out, "tp")
             gathered = (wide_rows + summed).astype(jnp.bfloat16)
         else:
             current = finish_split(partial_out, wide_rows)

time: 88.5 us -> 70.3 us (0.79)
  starting transfers between devices: 38.6 us -> 28.6 us
  local copies, waits for them, and re-layouts: 10.1 us -> 3.75 us
  other arithmetic: 12.9 us -> 10.4 us
  waiting for transfers between devices: 21.6 us -> 23.3 us
    ppermute x13 -> x6, starting transfers between devices: 17 us -> 7.61 us  [gather_direct(): lax.ppermute(rows, axis, [(j, (j - step) % size) for j in range(size)])]
    ppermute x7 -> x12, waiting for transfers between devices: 8.45 us -> 16.7 us  [the longest x3 6.01 us: sum_paired(): lax.ppermute(sent, axis, [(j, (j + step * inner) % size) for j in range(s...]
    ppermute x13 -> x6, starting transfers between devices: 16.8 us -> 8.6 us  [scatter_direct(): lax.ppermute(part, axis, [(j, (j + step) % size) for j in range(size)])]
    ppermute x7 -> x12, starting transfers between devices: 4.79 us -> 12.4 us  [the longest x3 5.74 us: gather_paired(): lax.ppermute(both, axis, [(j, (j - hop) % size) for j in range(size)])]
    unnamed x61 -> x33, local copies, waits for them, and re-layouts: 5.94 us -> 0.82 us
    ppermute x13 -> x6, waiting for transfers between devices: 7.1 us -> 2.48 us  [gather_direct(): lax.ppermute(rows, axis, [(j, (j - step) % size) for j in range(size)])]
    ppermute x13 -> x6, waiting for transfers between devices: 6.11 us -> 4.17 us  [scatter_direct(): lax.ppermute(part, axis, [(j, (j + step) % size) for j in range(size)])]
    reduce_sum x2, other arithmetic: 1.87 us -> 0.27 us  [body(): square_part = jnp.sum(wide_rows * wide_rows, axis=1)]
  transfers between devices with their start and end apart: 33 -> 24, of which waited for: 12 -> 15; matrix products, arithmetic and copies ran while one was open for 9% -> 8% of each run, Pallas kernels for 0% -> 0%
where the time goes in v2:
time: 70.3 us; the launch traced here: 70 us
  starting transfers between devices  28.6 us (41%)
  waiting for transfers between devices  23.3 us (33%)
  other arithmetic  10.4 us (15%)
  local copies, waits for them, and re-layouts  3.75 us (5%)
  matrix products  2.85 us (4%)
  between operations  1.1 us (2%)
    ppermute x6, starting transfers between devices, scatter_direct(): lax.ppermute(part, axis, [(j, (j + step) % size) for j in range(size)])  8.6 us
    ppermute x6, starting transfers between devices, gather_direct(): lax.ppermute(rows, axis, [(j, (j - step) % size) for j in range(size)])  7.61 us
    ppermute x3, waiting for transfers between devices, sum_paired(): lax.ppermute(sent, axis, [(j, (j + step * inner) % size) for j in range(s...  6.01 us
    ppermute x3, starting transfers between devices, gather_paired(): lax.ppermute(both, axis, [(j, (j - hop) % size) for j in range(size)])  5.74 us
    ppermute x3, waiting for transfers between devices, gather_paired(): lax.ppermute(both, axis, [(j, (j - hop) % size) for j in range(size)])  4.83 us
    ppermute x6, waiting for transfers between devices, scatter_direct(): lax.ppermute(part, axis, [(j, (j + step) % size) for j in range(size)])  4.17 us
    ppermute x3, waiting for transfers between devices, scatter_paired(): lax.ppermute(part, axis, [(j, (j + hop) % size) for j in range(size)])  3.98 us
    ppermute x3, starting transfers between devices, scatter_paired(): lax.ppermute(part, axis, [(j, (j + hop) % size) for j in range(size)])  3.87 us
  transfers between devices with their start and end apart: 24, of which 15 were waited for; matrix products, arithmetic and copies ran while one was open for 8% of the time, Pallas kernels for 0%

profile of v2, /device:TPU:0, one launch (start us, length us, event | category | flops | bytes accessed | tf_op | source)
XLA Modules:
  0.0 70.0 jit_solution(10676946299633663010)
XLA Ops:
  1.9 0.8 %slice_convert_fusion = (f32[1,1024]{1,0:T(1,128)S(1)}, f32[1,1024]{1,0:T(1,128)S(1)}) fusion(bf16[2,1024]{1,0:T(2,128)(2,1)} %param.13), kind=kLoop, calls=%fused_computation.177 | loop fusion | flops 2048 | bytes 12288 | tf_op jit(solution)/shard_map/mul | solution.py:161
  2.6 0.8 %fusion.113 = (bf16[1,1024,16]{1,2,0:T(8,128)(2,1)S(1)}, bf16[1,1024,16]{1,2,0:T(8,128)(2,1)S(1)}) fusion(bf16[2,1024,16]{1,2,0:T(8,128)(2,1)} %param.18), kind=kLoop, calls=%fused_computation.204 | loop fusion | bytes 131072 | tf_op jit(solution)/shard_map/slice | solution.py:164
  3.6 0.7 %broadcast_select_fusion.1 = (bf16[4,1024]{1,0:T(4,128)(2,1)S(1)}, bf16[4,1024]{1,0:T(4,128)(2,1)S(1)}) fusion(bf16[4,1024]{1,0:T(4,128)(2,1)} %param.12, bf16[4,1024]{1,0:T(4,128)(2,1)S(1)} %collective-permute-done, pred[]{:T(512)S(6)} %eq.16), kind=kLoop, calls=%fused_computation.112 | loop fusion | flops 8192 | bytes 32769 | tf_op jit(solution)/shard_map/jit(_where)/select_n | solution.py:81
  4.3 3.7 %collective-permute-start.2 = (bf16[8,1024]{1,0:T(8,128)(2,1)S(1)}, bf16[8,1024]{1,0:T(8,128)(2,1)S(1)}, u32[]{:S(2)}, u32[]{:S(2)}) collective-permute-start(bf16[8,1024]{1,0:T(8,128)(2,1)S(1)} %pad_maximum_fusion.1), channel_id=1, source_target_pairs={{0,16},{4,20},{8,24},{12,28},{16,0},{20,4},{24,8},{28,12},{1,17},{... | collective-permute-start | bytes 49160 | tf_op jit(solution)/shard_map/ppermute | solution.py:86
  8.0 1.3 %collective-permute-start.1 = (bf16[8,1024]{1,0:T(8,128)(2,1)S(1)}, bf16[8,1024]{1,0:T(8,128)(2,1)S(1)}, u32[]{:S(2)}, u32[]{:S(2)}) collective-permute-start(bf16[8,1024]{1,0:T(8,128)(2,1)S(1)} %pad_maximum_fusion.1), channel_id=1, source_target_pairs={{0,24},{4,28},{8,0},{12,4},{16,8},{20,12},{24,16},{28,20},{1,25},{... | collective-permute-start | bytes 49160 | tf_op jit(solution)/shard_map/ppermute | solution.py:86
  10.1 1.7 %collective-permute-done.1 = bf16[8,1024]{1,0:T(8,128)(2,1)S(1)} collective-permute-done((bf16[8,1024]{1,0:T(8,128)(2,1)S(1)}, bf16[8,1024]{1,0:T(8,128)(2,1)S(1)}, u32[]{:S(2)}, u32[]{:S(2)}) %collective-permute-start.1) | collective-permute-done | bytes 16416 | tf_op jit(solution)/shard_map/ppermute | solution.py:86
  11.8 3.1 %collective-permute-done.3 = bf16[8,1024]{1,0:T(8,128)(2,1)S(1)} collective-permute-done((bf16[8,1024]{1,0:T(8,128)(2,1)S(1)}, bf16[8,1024]{1,0:T(8,128)(2,1)S(1)}, u32[]{:S(2)}, u32[]{:S(2)}) %collective-permute-start.3) | collective-permute-done | bytes 16416 | tf_op jit(solution)/shard_map/ppermute | solution.py:86
  15.6 1.1 %fusion.18 = f32[4,8,128]{2,1,0:T(8,128)S(1)} fusion(bf16[2,1024,128]{2,1,0:T(8,128)(2,1)} %param.17, f32[1024]{0:T(1024)S(1)} %bitcast.226, bf16[8,8,1024]{2,1,0:T(8,128)(2,1)S(1)} %constant_dynamic-update-slice_fusion, s32[]{:T(128)S(6)} %select_n.125), kind=kOutput, calls=%fused_computation.24 | convolution fusion | flops 8486912 | bytes 348164 | tf_op jit(solution)/shard_map/dot_general | solution.py:175
  17.1 1.5 %collective-permute-start.4 = (f32[8,515]{1,0:T(8,128)S(1)}, f32[8,515]{1,0:T(8,128)S(1)}, u32[]{:S(2)}, u32[]{:S(2)}) collective-permute-start(f32[8,515]{1,0:T(8,128)S(1)} %get-tuple-element.47), channel_id=1, source_target_pairs={{0,1},{1,2},{2,3},{3,0},{4,5},{5,6},{6,7},{7,4},{8,9},{9,10},{10,1... | collective-permute-start | bytes 49448 | tf_op jit(solution)/shard_map/ppermute | solution.py:59
  18.7 1.4 %collective-permute-start.6 = (f32[8,515]{1,0:T(8,128)S(1)}, f32[8,515]{1,0:T(8,128)S(1)}, u32[]{:S(2)}, u32[]{:S(2)}) collective-permute-start(f32[8,515]{1,0:T(8,128)S(1)} %get-tuple-element.48), channel_id=1, source_target_pairs={{0,3},{1,0},{2,1},{3,2},{4,7},{5,4},{6,5},{7,6},{8,11},{9,8},{10,9... | collective-permute-start | bytes 49448 | tf_op jit(solution)/shard_map/ppermute | solution.py:59
  20.1 1.5 %collective-permute-start.5 = (f32[8,515]{1,0:T(8,128)S(1)}, f32[8,515]{1,0:T(8,128)S(1)}, u32[]{:S(2)}, u32[]{:S(2)}) collective-permute-start(f32[8,515]{1,0:T(8,128)S(1)} %get-tuple-element.49), channel_id=1, source_target_pairs={{0,2},{1,3},{2,0},{3,1},{4,6},{5,7},{6,4},{7,5},{8,10},{9,11},{10,... | collective-permute-start | bytes 49448 | tf_op jit(solution)/shard_map/ppermute | solution.py:59
  22.4 1.4 %collective-permute-done.5 = f32[8,515]{1,0:T(8,128)S(1)} collective-permute-done((f32[8,515]{1,0:T(8,128)S(1)}, f32[8,515]{1,0:T(8,128)S(1)}, u32[]{:S(2)}, u32[]{:S(2)}) %collective-permute-start.5) | collective-permute-done | bytes 16512 | tf_op jit(solution)/shard_map/ppermute | solution.py:59
  24.2 1.5 %exponential_reduce_fusion.3 = (f32[8]{0:T(128)S(1)}, f32[8]{0:T(128)S(1)}, f32[8,1]{1,0:T(8,128)S(1)}) fusion(f32[8,1]{1,0:T(8,128)S(1)} %copy.47, f32[]{:T(128)} %bitcast.22, f32[8,2]{1,0:T(8,128)S(1)} %slice_multiply_fusion.9, f32[]{:T(128)} %bitcast.24), kind=kLoop, calls=%fused_computation.183 | loop fusion | flops 112 | bytes 200 | tf_op jit(solution)/shard_map/exp | solution.py:23
  26.7 1.6 %collective-permute-start.7 = (bf16[8,128]{1,0:T(8,128)(2,1)S(1)}, bf16[8,128]{1,0:T(8,128)(2,1)S(1)}, u32[]{:S(2)}, u32[]{:S(2)}) collective-permute-start(bf16[8,128]{1,0:T(8,128)(2,1)S(1)} %get-tuple-element.38), channel_id=1, source_target_pairs={{0,3},{1,0},{2,1},{3,2},{4,7},{5,4},{6,5},{7,6},{8,11},{9,8},{10,9... | collective-permute-start | bytes 6152 | tf_op jit(solution)/shard_map/ppermute | solution.py:46
  28.7 1.5 %collective-permute-start.8 = (bf16[8,128]{1,0:T(8,128)(2,1)S(1)}, bf16[8,128]{1,0:T(8,128)(2,1)S(1)}, u32[]{:S(2)}, u32[]{:S(2)}) collective-permute-start(bf16[8,128]{1,0:T(8,128)(2,1)S(1)} %get-tuple-element.38), channel_id=1, source_target_pairs={{0,2},{1,3},{2,0},{3,1},{4,6},{5,7},{6,4},{7,5},{8,10},{9,11},{10,... | collective-permute-start | bytes 6152 | tf_op jit(solution)/shard_map/ppermute | solution.py:46
  30.3 2.0 %collective-permute-done.8 = bf16[8,128]{1,0:T(8,128)(2,1)S(1)} collective-permute-done((bf16[8,128]{1,0:T(8,128)(2,1)S(1)}, bf16[8,128]{1,0:T(8,128)(2,1)S(1)}, u32[]{:S(2)}, u32[]{:S(2)}) %collective-permute-start.8) | collective-permute-done | bytes 2080 | tf_op jit(solution)/shard_map/ppermute | solution.py:46
  33.0 1.2 %collective-permute-done.10 = bf16[32,1024]{1,0:T(8,128)(2,1)S(1)} collective-permute-done((bf16[32,1024]{1,0:T(8,128)(2,1)S(1)}, bf16[32,1024]{1,0:T(8,128)(2,1)S(1)}, u32[]{:S(2)}, u32[]{:S(2)}) %collective-permute-start.10) | collective-permute-done | bytes 65568 | tf_op jit(solution)/shard_map/ppermute | solution.py:72
  34.7 1.7 %collective-permute-start.11 = (bf16[32,1024]{1,0:T(8,128)(2,1)S(1)}, bf16[32,1024]{1,0:T(8,128)(2,1)S(1)}, u32[]{:S(2)}, u32[]{:S(2)}) collective-permute-start(bf16[32,1024]{1,0:T(8,128)(2,1)S(1)} %fusion.40), channel_id=1, source_target_pairs={{0,8},{4,12},{8,16},{12,20},{16,24},{20,28},{24,0},{28,4},{1,9},{5... | collective-permute-start | bytes 196616 | tf_op jit(solution)/shard_map/ppermute | solution.py:99
  36.4 3.3 %collective-permute-done.13 = bf16[32,1024]{1,0:T(8,128)(2,1)S(1)} collective-permute-done((bf16[32,1024]{1,0:T(8,128)(2,1)S(1)}, bf16[32,1024]{1,0:T(8,128)(2,1)S(1)}, u32[]{:S(2)}, u32[]{:S(2)}) %collective-permute-start.13) | collective-permute-done | bytes 65568 | tf_op jit(solution)/shard_map/ppermute | solution.py:99
  39.7 2.7 %collective-permute-done.12 = bf16[32,1024]{1,0:T(8,128)(2,1)S(1)} collective-permute-done((bf16[32,1024]{1,0:T(8,128)(2,1)S(1)}, bf16[32,1024]{1,0:T(8,128)(2,1)S(1)}, u32[]{:S(2)}, u32[]{:S(2)}) %collective-permute-start.12) | collective-permute-done | bytes 65568 | tf_op jit(solution)/shard_map/ppermute | solution.py:99
  44.3 1.5 %collective-permute-start.14 = (f32[8,515]{1,0:T(8,128)S(1)}, f32[8,515]{1,0:T(8,128)S(1)}, u32[]{:S(2)}, u32[]{:S(2)}) collective-permute-start(f32[8,515]{1,0:T(8,128)S(1)} %get-tuple-element.44), channel_id=1, source_target_pairs={{0,1},{1,2},{2,3},{3,0},{4,5},{5,6},{6,7},{7,4},{8,9},{9,10},{10,1... | collective-permute-start | bytes 49448 | tf_op jit(solution)/shard_map/ppermute | solution.py:59
  45.8 1.5 %collective-permute-start.16 = (f32[8,515]{1,0:T(8,128)S(1)}, f32[8,515]{1,0:T(8,128)S(1)}, u32[]{:S(2)}, u32[]{:S(2)}) collective-permute-start(f32[8,515]{1,0:T(8,128)S(1)} %get-tuple-element.45), channel_id=1, source_target_pairs={{0,3},{1,0},{2,1},{3,2},{4,7},{5,4},{6,5},{7,6},{8,11},{9,8},{10,9... | collective-permute-start | bytes 49448 | tf_op jit(solution)/shard_map/ppermute | solution.py:59
  47.2 1.1 %collective-permute-start.15 = (f32[8,515]{1,0:T(8,128)S(1)}, f32[8,515]{1,0:T(8,128)S(1)}, u32[]{:S(2)}, u32[]{:S(2)}) collective-permute-start(f32[8,515]{1,0:T(8,128)S(1)} %get-tuple-element.46), channel_id=1, source_target_pairs={{0,2},{1,3},{2,0},{3,1},{4,6},{5,7},{6,4},{7,5},{8,10},{9,11},{10,... | collective-permute-start | bytes 49448 | tf_op jit(solution)/shard_map/ppermute | solution.py:59
  49.6 1.5 %collective-permute-done.15 = f32[8,515]{1,0:T(8,128)S(1)} collective-permute-done((f32[8,515]{1,0:T(8,128)S(1)}, f32[8,515]{1,0:T(8,128)S(1)}, u32[]{:S(2)}, u32[]{:S(2)}) %collective-permute-start.15) | collective-permute-done | bytes 16512 | tf_op jit(solution)/shard_map/ppermute | solution.py:59
  51.3 1.5 %exponential_reduce_fusion.1 = (f32[8]{0:T(128)S(1)}, f32[8]{0:T(128)S(1)}, f32[8,1]{1,0:T(8,128)S(1)}) fusion(f32[8,1]{1,0:T(8,128)S(1)} %copy.52, f32[]{:T(128)} %bitcast.52, f32[8,2]{1,0:T(8,128)S(1)} %slice_multiply_fusion.3, f32[]{:T(128)} %bitcast.54), kind=kLoop, calls=%fused_computation.175 | loop fusion | flops 112 | bytes 200 | tf_op jit(solution)/shard_map/exp | solution.py:23
  53.8 0.8 %collective-permute-start.19 = (bf16[8,128]{1,0:T(8,128)(2,1)S(1)}, bf16[8,128]{1,0:T(8,128)(2,1)S(1)}, u32[]{:S(2)}, u32[]{:S(2)}) collective-permute-start(bf16[8,128]{1,0:T(8,128)(2,1)S(1)} %get-tuple-element.31), channel_id=1, source_target_pairs={{0,1},{1,2},{2,3},{3,0},{4,5},{5,6},{6,7},{7,4},{8,9},{9,10},{10,1... | collective-permute-start | bytes 6152 | tf_op jit(solution)/shard_map/ppermute | solution.py:46
  54.6 0.9 %collective-permute-start.18 = (bf16[8,128]{1,0:T(8,128)(2,1)S(1)}, bf16[8,128]{1,0:T(8,128)(2,1)S(1)}, u32[]{:S(2)}, u32[]{:S(2)}) collective-permute-start(bf16[8,128]{1,0:T(8,128)(2,1)S(1)} %get-tuple-element.31), channel_id=1, source_target_pairs={{0,2},{1,3},{2,0},{3,1},{4,6},{5,7},{6,4},{7,5},{8,10},{9,11},{10,... | collective-permute-start | bytes 6152 | tf_op jit(solution)/shard_map/ppermute | solution.py:46
  55.5 2.3 %collective-permute-start.17 = (bf16[8,128]{1,0:T(8,128)(2,1)S(1)}, bf16[8,128]{1,0:T(8,128)(2,1)S(1)}, u32[]{:S(2)}, u32[]{:S(2)}) collective-permute-start(bf16[8,128]{1,0:T(8,128)(2,1)S(1)} %get-tuple-element.31), channel_id=1, source_target_pairs={{0,3},{1,0},{2,1},{3,2},{4,7},{5,4},{6,5},{7,6},{8,11},{9,8},{10,9... | collective-permute-start | bytes 6152 | tf_op jit(solution)/shard_map/ppermute | solution.py:46
  58.3 1.0 %pad_maximum_fusion = f32[2,8,1,128,128]{4,3,2,1,0:T(8,128)} fusion(f32[1,8,1,128,128]{4,3,2,1,0:T(8,128)S(1)} %get-tuple-element.43, f32[1,8,1,128,128]{4,3,2,1,0:T(8,128)S(1)} %get-tuple-element.42), kind=kLoop, calls=%fused_computation.1 | loop fusion | flops 262144 | bytes 2097152 | tf_op jit(solution)/shard_map/stack | solution.py:225
  61.0 3.8 %collective-permute-start.23 = (bf16[4,1024]{1,0:T(4,128)(2,1)S(1)}, bf16[4,1024]{1,0:T(4,128)(2,1)S(1)}, u32[]{:S(2)}, u32[]{:S(2)}) collective-permute-start(bf16[4,1024]{1,0:T(4,128)(2,1)S(1)} %get-tuple-element.53), channel_id=1, source_target_pairs={{0,24},{4,28},{8,0},{12,4},{16,8},{20,12},{24,16},{28,20},{1,25},{... | collective-permute-start | bytes 24584 | tf_op jit(solution)/shard_map/ppermute | solution.py:120
  65.4 1.1 %collective-permute-done.21 = bf16[4,1024]{1,0:T(4,128)(2,1)S(1)} collective-permute-done((bf16[4,1024]{1,0:T(4,128)(2,1)S(1)}, bf16[4,1024]{1,0:T(4,128)(2,1)S(1)}, u32[]{:S(2)}, u32[]{:S(2)}) %collective-permute-start.21) | collective-permute-done | bytes 8224 | tf_op jit(solution)/shard_map/ppermute | solution.py:120
  66.5 2.9 %collective-permute-done.22 = bf16[4,1024]{1,0:T(4,128)(2,1)S(1)} collective-permute-done((bf16[4,1024]{1,0:T(4,128)(2,1)S(1)}, bf16[4,1024]{1,0:T(4,128)(2,1)S(1)}, u32[]{:S(2)}, u32[]{:S(2)}) %collective-permute-start.22) | collective-permute-done | bytes 8224 | tf_op jit(solution)/shard_map/ppermute | solution.py:120
  (119 shorter events, 14.2 us)
Async XLA Ops:
  0.6 14.6 %copy-start.1 = (bf16[2,1024,128]{2,1,0:T(8,128)(2,1)S(1)}, bf16[2,1024,128]{2,1,0:T(8,128)(2,1)}, u32[]{:S(2)}) copy-start(bf16[2,1024,128]{2,1,0:T(8,128)(2,1)} %param.15) | copy-start | bytes 1572868
  0.6 2.9 %collective-permute-start = (bf16[4,1024]{1,0:T(4,128)(2,1)}, bf16[4,1024]{1,0:T(4,128)(2,1)S(1)}, u32[]{:S(2)}, u32[]{:S(2)}) collective-permute-start(bf16[4,1024]{1,0:T(4,128)(2,1)} %param.12), channel_id=1, source_target_pairs={{0,4},{4,0},{8,12},{12,8},{16,20},{20,16},{24,28},{28,24},{1,5},{5... | collective-permute-start | bytes 24584 | tf_op jit(solution)/shard_map/ppermute | solution.py:72
  2.6 12.7 %copy-start.2 = (bf16[2,1024,128]{2,1,0:T(8,128)(2,1)S(1)}, bf16[2,1024,128]{2,1,0:T(8,128)(2,1)}, u32[]{:S(2)}) copy-start(bf16[2,1024,128]{2,1,0:T(8,128)(2,1)} %param.16) | copy-start | bytes 1572868
  4.3 7.5 %collective-permute-start.2 = (bf16[8,1024]{1,0:T(8,128)(2,1)S(1)}, bf16[8,1024]{1,0:T(8,128)(2,1)S(1)}, u32[]{:S(2)}, u32[]{:S(2)}) collective-permute-start(bf16[8,1024]{1,0:T(8,128)(2,1)S(1)} %pad_maximum_fusion.1), channel_id=1, source_target_pairs={{0,16},{4,20},{8,24},{12,28},{16,0},{20,4},{24,8},{28,12},{1,17},{... | collective-permute-start | bytes 49160 | tf_op jit(solution)/shard_map/ppermute | solution.py:86
  8.0 3.7 %collective-permute-start.1 = (bf16[8,1024]{1,0:T(8,128)(2,1)S(1)}, bf16[8,1024]{1,0:T(8,128)(2,1)S(1)}, u32[]{:S(2)}, u32[]{:S(2)}) collective-permute-start(bf16[8,1024]{1,0:T(8,128)(2,1)S(1)} %pad_maximum_fusion.1), channel_id=1, source_target_pairs={{0,24},{4,28},{8,0},{12,4},{16,8},{20,12},{24,16},{28,20},{1,25},{... | collective-permute-start | bytes 49160 | tf_op jit(solution)/shard_map/ppermute | solution.py:86
  9.4 5.5 %collective-permute-start.3 = (bf16[8,1024]{1,0:T(8,128)(2,1)S(1)}, bf16[8,1024]{1,0:T(8,128)(2,1)S(1)}, u32[]{:S(2)}, u32[]{:S(2)}) collective-permute-start(bf16[8,1024]{1,0:T(8,128)(2,1)S(1)} %pad_maximum_fusion.1), channel_id=1, source_target_pairs={{0,8},{4,12},{8,16},{12,20},{16,24},{20,28},{24,0},{28,4},{1,9},{5... | collective-permute-start | bytes 49160 | tf_op jit(solution)/shard_map/ppermute | solution.py:86
  15.0 1.7 %copy-start.4 = (bf16[2,1024,128]{2,1,0:T(8,128)(2,1)S(1)}, bf16[2,1024,128]{2,1,0:T(8,128)(2,1)}, u32[]{:S(2)}) copy-start(bf16[2,1024,128]{2,1,0:T(8,128)(2,1)} %param.14) | copy-start | bytes 1572868
  15.0 6.6 %copy-start.7 = (f32[2,2,1]{1,2,0:T(1,128)S(1)}, f32[2,2,1]{1,2,0:T(1,128)}, u32[]{:S(2)}) copy-start(f32[2,2,1]{1,2,0:T(1,128)} %param.19) | copy-start | bytes 52
  15.1 11.1 %copy-start = (f32[2,8,1,128,128]{4,3,2,1,0:T(8,128)S(1)}, f32[2,8,1,128,128]{4,3,2,1,0:T(8,128)}, u32[]{:S(2)}) copy-start(f32[2,8,1,128,128]{4,3,2,1,0:T(8,128)} %param.21) | copy-start | bytes 3145732
  17.0 8.7 %copy-start.6 = (f32[2,8,1,128]{3,2,1,0:T(1,128)S(1)}, f32[2,8,1,128]{3,2,1,0:T(1,128)}, u32[]{:S(2)}) copy-start(f32[2,8,1,128]{3,2,1,0:T(1,128)} %param.22) | copy-start | bytes 24580
  17.1 15.7 %copy-start.5 = (bf16[2,128,1024]{2,1,0:T(8,128)(2,1)S(1)}, bf16[2,128,1024]{2,1,0:T(8,128)(2,1)}, u32[]{:S(2)}) copy-start(bf16[2,128,1024]{2,1,0:T(8,128)(2,1)} %param.20) | copy-start | bytes 1572868
  17.1 5.2 %collective-permute-start.4 = (f32[8,515]{1,0:T(8,128)S(1)}, f32[8,515]{1,0:T(8,128)S(1)}, u32[]{:S(2)}, u32[]{:S(2)}) collective-permute-start(f32[8,515]{1,0:T(8,128)S(1)} %get-tuple-element.47), channel_id=1, source_target_pairs={{0,1},{1,2},{2,3},{3,0},{4,5},{5,6},{6,7},{7,4},{8,9},{9,10},{10,1... | collective-permute-start | bytes 49448 | tf_op jit(solution)/shard_map/ppermute | solution.py:59
  18.7 3.8 %collective-permute-start.6 = (f32[8,515]{1,0:T(8,128)S(1)}, f32[8,515]{1,0:T(8,128)S(1)}, u32[]{:S(2)}, u32[]{:S(2)}) collective-permute-start(f32[8,515]{1,0:T(8,128)S(1)} %get-tuple-element.48), channel_id=1, source_target_pairs={{0,3},{1,0},{2,1},{3,2},{4,7},{5,4},{6,5},{7,6},{8,11},{9,8},{10,9... | collective-permute-start | bytes 49448 | tf_op jit(solution)/shard_map/ppermute | solution.py:59
  20.1 3.8 %collective-permute-start.5 = (f32[8,515]{1,0:T(8,128)S(1)}, f32[8,515]{1,0:T(8,128)S(1)}, u32[]{:S(2)}, u32[]{:S(2)}) collective-permute-start(f32[8,515]{1,0:T(8,128)S(1)} %get-tuple-element.49), channel_id=1, source_target_pairs={{0,2},{1,3},{2,0},{3,1},{4,6},{5,7},{6,4},{7,5},{8,10},{9,11},{10,... | collective-permute-start | bytes 49448 | tf_op jit(solution)/shard_map/ppermute | solution.py:59
  26.7 3.6 %collective-permute-start.7 = (bf16[8,128]{1,0:T(8,128)(2,1)S(1)}, bf16[8,128]{1,0:T(8,128)(2,1)S(1)}, u32[]{:S(2)}, u32[]{:S(2)}) collective-permute-start(bf16[8,128]{1,0:T(8,128)(2,1)S(1)} %get-tuple-element.38), channel_id=1, source_target_pairs={{0,3},{1,0},{2,1},{3,2},{4,7},{5,4},{6,5},{7,6},{8,11},{9,8},{10,9... | collective-permute-start | bytes 6152 | tf_op jit(solution)/shard_map/ppermute | solution.py:46
  28.2 4.5 %collective-permute-start.9 = (bf16[8,128]{1,0:T(8,128)(2,1)S(1)}, bf16[8,128]{1,0:T(8,128)(2,1)S(1)}, u32[]{:S(2)}, u32[]{:S(2)}) collective-permute-start(bf16[8,128]{1,0:T(8,128)(2,1)S(1)} %get-tuple-element.38), channel_id=1, source_target_pairs={{0,1},{1,2},{2,3},{3,0},{4,5},{5,6},{6,7},{7,4},{8,9},{9,10},{10,1... | collective-permute-start | bytes 6152 | tf_op jit(solution)/shard_map/ppermute | solution.py:46
  28.7 3.6 %collective-permute-start.8 = (bf16[8,128]{1,0:T(8,128)(2,1)S(1)}, bf16[8,128]{1,0:T(8,128)(2,1)S(1)}, u32[]{:S(2)}, u32[]{:S(2)}) collective-permute-start(bf16[8,128]{1,0:T(8,128)(2,1)S(1)} %get-tuple-element.38), channel_id=1, source_target_pairs={{0,2},{1,3},{2,0},{3,1},{4,6},{5,7},{6,4},{7,5},{8,10},{9,11},{10,... | collective-permute-start | bytes 6152 | tf_op jit(solution)/shard_map/ppermute | solution.py:46
  32.9 1.3 %collective-permute-start.10 = (bf16[32,1024]{1,0:T(8,128)(2,1)S(1)}, bf16[32,1024]{1,0:T(8,128)(2,1)S(1)}, u32[]{:S(2)}, u32[]{:S(2)}) collective-permute-start(bf16[32,1024]{1,0:T(8,128)(2,1)S(1)} %get-tuple-element.73), channel_id=1, source_target_pairs={{0,4},{4,0},{8,12},{12,8},{16,20},{20,16},{24,28},{28,24},{1,5},{5... | collective-permute-start | bytes 196616 | tf_op jit(solution)/shard_map/ppermute | solution.py:72
  34.3 5.4 %collective-permute-start.13 = (bf16[32,1024]{1,0:T(8,128)(2,1)S(1)}, bf16[32,1024]{1,0:T(8,128)(2,1)S(1)}, u32[]{:S(2)}, u32[]{:S(2)}) collective-permute-start(bf16[32,1024]{1,0:T(8,128)(2,1)S(1)} %fusion.40), channel_id=1, source_target_pairs={{0,24},{4,28},{8,0},{12,4},{16,8},{20,12},{24,16},{28,20},{1,25},{... | collective-permute-start | bytes 196616 | tf_op jit(solution)/shard_map/ppermute | solution.py:99
  34.4 8.0 %collective-permute-start.12 = (bf16[32,1024]{1,0:T(8,128)(2,1)S(1)}, bf16[32,1024]{1,0:T(8,128)(2,1)S(1)}, u32[]{:S(2)}, u32[]{:S(2)}) collective-permute-start(bf16[32,1024]{1,0:T(8,128)(2,1)S(1)} %fusion.40), channel_id=1, source_target_pairs={{0,16},{4,20},{8,24},{12,28},{16,0},{20,4},{24,8},{28,12},{1,17},{... | collective-permute-start | bytes 196616 | tf_op jit(solution)/shard_map/ppermute | solution.py:99
  34.7 7.7 %collective-permute-start.11 = (bf16[32,1024]{1,0:T(8,128)(2,1)S(1)}, bf16[32,1024]{1,0:T(8,128)(2,1)S(1)}, u32[]{:S(2)}, u32[]{:S(2)}) collective-permute-start(bf16[32,1024]{1,0:T(8,128)(2,1)S(1)} %fusion.40), channel_id=1, source_target_pairs={{0,8},{4,12},{8,16},{12,20},{16,24},{20,28},{24,0},{28,4},{1,9},{5... | collective-permute-start | bytes 196616 | tf_op jit(solution)/shard_map/ppermute | solution.py:99
  42.5 1.0 %copy-start.3 = (bf16[2,1024,128]{2,1,0:T(8,128)(2,1)S(1)}, bf16[2,1024,128]{2,1,0:T(8,128)(2,1)}, u32[]{:S(2)}) copy-start(bf16[2,1024,128]{2,1,0:T(8,128)(2,1)} %param.17) | copy-start | bytes 1572868
  44.3 4.7 %collective-permute-start.14 = (f32[8,515]{1,0:T(8,128)S(1)}, f32[8,515]{1,0:T(8,128)S(1)}, u32[]{:S(2)}, u32[]{:S(2)}) collective-permute-start(f32[8,515]{1,0:T(8,128)S(1)} %get-tuple-element.44), channel_id=1, source_target_pairs={{0,1},{1,2},{2,3},{3,0},{4,5},{5,6},{6,7},{7,4},{8,9},{9,10},{10,1... | collective-permute-start | bytes 49448 | tf_op jit(solution)/shard_map/ppermute | solution.py:59
  45.8 3.8 %collective-permute-start.16 = (f32[8,515]{1,0:T(8,128)S(1)}, f32[8,515]{1,0:T(8,128)S(1)}, u32[]{:S(2)}, u32[]{:S(2)}) collective-permute-start(f32[8,515]{1,0:T(8,128)S(1)} %get-tuple-element.45), channel_id=1, source_target_pairs={{0,3},{1,0},{2,1},{3,2},{4,7},{5,4},{6,5},{7,6},{8,11},{9,8},{10,9... | collective-permute-start | bytes 49448 | tf_op jit(solution)/shard_map/ppermute | solution.py:59
  47.2 3.8 %collective-permute-start.15 = (f32[8,515]{1,0:T(8,128)S(1)}, f32[8,515]{1,0:T(8,128)S(1)}, u32[]{:S(2)}, u32[]{:S(2)}) collective-permute-start(f32[8,515]{1,0:T(8,128)S(1)} %get-tuple-element.46), channel_id=1, source_target_pairs={{0,2},{1,3},{2,0},{3,1},{4,6},{5,7},{6,4},{7,5},{8,10},{9,11},{10,... | collective-permute-start | bytes 49448 | tf_op jit(solution)/shard_map/ppermute | solution.py:59
  53.8 5.5 %collective-permute-start.19 = (bf16[8,128]{1,0:T(8,128)(2,1)S(1)}, bf16[8,128]{1,0:T(8,128)(2,1)S(1)}, u32[]{:S(2)}, u32[]{:S(2)}) collective-permute-start(bf16[8,128]{1,0:T(8,128)(2,1)S(1)} %get-tuple-element.31), channel_id=1, source_target_pairs={{0,1},{1,2},{2,3},{3,0},{4,5},{5,6},{6,7},{7,4},{8,9},{9,10},{10,1... | collective-permute-start | bytes 6152 | tf_op jit(solution)/shard_map/ppermute | solution.py:46
  54.6 4.7 %collective-permute-start.18 = (bf16[8,128]{1,0:T(8,128)(2,1)S(1)}, bf16[8,128]{1,0:T(8,128)(2,1)S(1)}, u32[]{:S(2)}, u32[]{:S(2)}) collective-permute-start(bf16[8,128]{1,0:T(8,128)(2,1)S(1)} %get-tuple-element.31), channel_id=1, source_target_pairs={{0,2},{1,3},{2,0},{3,1},{4,6},{5,7},{6,4},{7,5},{8,10},{9,11},{10,... | collective-permute-start | bytes 6152 | tf_op jit(solution)/shard_map/ppermute | solution.py:46
  55.5 3.8 %collective-permute-start.17 = (bf16[8,128]{1,0:T(8,128)(2,1)S(1)}, bf16[8,128]{1,0:T(8,128)(2,1)S(1)}, u32[]{:S(2)}, u32[]{:S(2)}) collective-permute-start(bf16[8,128]{1,0:T(8,128)(2,1)S(1)} %get-tuple-element.31), channel_id=1, source_target_pairs={{0,3},{1,0},{2,1},{3,2},{4,7},{5,4},{6,5},{7,6},{8,11},{9,8},{10,9... | collective-permute-start | bytes 6152 | tf_op jit(solution)/shard_map/ppermute | solution.py:46
  59.6 1.3 %collective-permute-start.20 = (bf16[4,4,1024]{2,1,0:T(4,128)(2,1)S(1)}, bf16[4,4,1024]{2,1,0:T(4,128)(2,1)S(1)}, u32[]{:S(2)}, u32[]{:S(2)}) collective-permute-start(bf16[4,4,1024]{2,1,0:T(4,128)(2,1)S(1)} %fusion.46), channel_id=1, source_target_pairs={{0,4},{4,0},{8,12},{12,8},{16,20},{20,16},{24,28},{28,24},{1,5},{5... | collective-permute-start | bytes 98312 | tf_op jit(solution)/shard_map/ppermute | solution.py:72
  61.0 5.5 %collective-permute-start.21 = (bf16[4,1024]{1,0:T(4,128)(2,1)S(1)}, bf16[4,1024]{1,0:T(4,128)(2,1)S(1)}, u32[]{:S(2)}, u32[]{:S(2)}) collective-permute-start(bf16[4,1024]{1,0:T(4,128)(2,1)S(1)} %get-tuple-element.52), channel_id=1, source_target_pairs={{0,8},{4,12},{8,16},{12,20},{16,24},{20,28},{24,0},{28,4},{1,9},{5... | collective-permute-start | bytes 24584 | tf_op jit(solution)/shard_map/ppermute | solution.py:120
  61.0 5.4 %collective-permute-start.23 = (bf16[4,1024]{1,0:T(4,128)(2,1)S(1)}, bf16[4,1024]{1,0:T(4,128)(2,1)S(1)}, u32[]{:S(2)}, u32[]{:S(2)}) collective-permute-start(bf16[4,1024]{1,0:T(4,128)(2,1)S(1)} %get-tuple-element.53), channel_id=1, source_target_pairs={{0,24},{4,28},{8,0},{12,4},{16,8},{20,12},{24,16},{28,20},{1,25},{... | collective-permute-start | bytes 24584 | tf_op jit(solution)/shard_map/ppermute | solution.py:120
  64.8 4.5 %collective-permute-start.22 = (bf16[4,1024]{1,0:T(4,128)(2,1)S(1)}, bf16[4,1024]{1,0:T(4,128)(2,1)S(1)}, u32[]{:S(2)}, u32[]{:S(2)}) collective-permute-start(bf16[4,1024]{1,0:T(4,128)(2,1)S(1)} %get-tuple-element.54), channel_id=1, source_target_pairs={{0,16},{4,20},{8,24},{12,28},{16,0},{20,4},{24,8},{28,12},{1,17},{... | collective-permute-start | bytes 24584 | tf_op jit(solution)/shard_map/ppermute | solution.py:120

commit v3 on v2

--- a/solution.py
+++ b/solution.py
@@ -90,16 +90,13 @@
 
 
 def sum_paired(term, axis):
-    size, inner, groups, _, _ = pairing(axis)
+    size = lax.axis_size(axis)
+    if size & (size - 1):
+        return lax.psum(term, axis)
     total = term
-    if inner == 2:
-        total = total + swap(term.astype(jnp.bfloat16), axis, size).astype(jnp.float32)
-    sent = total.astype(jnp.bfloat16)
-    received = [
-        lax.ppermute(sent, axis, [(j, (j + step * inner) % size) for j in range(size)])
-        for step in range(1, groups)
-    ]
-    for part in received:
+    for mask in [1] + [2 * (2 << bit) - 2 for bit in range(size.bit_length() - 2)]:
+        sent = total.astype(jnp.bfloat16)
+        part = lax.ppermute(sent, axis, [(j, j ^ mask) for j in range(size)])
         total = total + part.astype(jnp.float32)
     return total
 

time: 70.3 us -> 72.7 us (1.034)
  waiting for transfers between devices: 23.3 us -> 27.6 us
  starting transfers between devices: 28.6 us -> 26.7 us
    ppermute x3, waiting for transfers between devices: 6.01 us -> 11.5 us  [sum_paired(): part = lax.ppermute(sent, axis, [(j, j ^ mask) for j in range(size)])]
    ppermute x3, starting transfers between devices: 2.08 us -> 0.25 us  [sum_paired(): part = lax.ppermute(sent, axis, [(j, j ^ mask) for j in range(size)])]
    ppermute x3 -> x2, waiting for transfers between devices: 1.84 us -> 0.59 us  [swap(): return lax.ppermute(value, axis, [(j, j ^ 1) for j in range(size)])]
  transfers between devices with their start and end apart: 24 -> 23, of which waited for: 15 -> 15; matrix products, arithmetic and copies ran while one was open for 8% -> 8% of each run, Pallas kernels for 0% -> 0%
where the time goes in v3:
time: 72.7 us; the launch traced here: 72.4 us
  waiting for transfers between devices  27.6 us (38%)
  starting transfers between devices  26.7 us (37%)
  other arithmetic  10.4 us (14%)
  local copies, waits for them, and re-layouts  3.75 us (5%)
  matrix products  2.85 us (4%)
  between operations  1.11 us (2%)
    ppermute x3, waiting for transfers between devices, sum_paired(): part = lax.ppermute(sent, axis, [(j, j ^ mask) for j in range(size)])  11.5 us
    ppermute x6, starting transfers between devices, scatter_direct(): lax.ppermute(part, axis, [(j, (j + step) % size) for j in range(size)])  8.6 us
    ppermute x6, starting transfers between devices, gather_direct(): lax.ppermute(rows, axis, [(j, (j - step) % size) for j in range(size)])  7.61 us
    ppermute x3, starting transfers between devices, gather_paired(): lax.ppermute(both, axis, [(j, (j - hop) % size) for j in range(size)])  5.74 us
    ppermute x3, waiting for transfers between devices, gather_paired(): lax.ppermute(both, axis, [(j, (j - hop) % size) for j in range(size)])  4.83 us
    ppermute x6, waiting for transfers between devices, scatter_direct(): lax.ppermute(part, axis, [(j, (j + step) % size) for j in range(size)])  4.17 us
    ppermute x3, waiting for transfers between devices, scatter_paired(): lax.ppermute(part, axis, [(j, (j + hop) % size) for j in range(size)])  3.98 us
    ppermute x3, starting transfers between devices, scatter_paired(): lax.ppermute(part, axis, [(j, (j + hop) % size) for j in range(size)])  3.87 us
  transfers between devices with their start and end apart: 23, of which 15 were waited for; matrix products, arithmetic and copies ran while one was open for 8% of the time, Pallas kernels for 0%

profile of v3, /device:TPU:0, one launch (start us, length us, event | category | flops | bytes accessed | tf_op | source)
XLA Modules:
  0.0 72.4 jit_solution(1441509755057721085)
XLA Ops:
  1.9 0.8 %slice_convert_fusion = (f32[1,1024]{1,0:T(1,128)S(1)}, f32[1,1024]{1,0:T(1,128)S(1)}) fusion(bf16[2,1024]{1,0:T(2,128)(2,1)} %param.13), kind=kLoop, calls=%fused_computation.179 | loop fusion | flops 2048 | bytes 12288 | tf_op jit(solution)/shard_map/mul | solution.py:158
  2.6 0.8 %fusion.114 = (bf16[1,1024,16]{1,2,0:T(8,128)(2,1)S(1)}, bf16[1,1024,16]{1,2,0:T(8,128)(2,1)S(1)}) fusion(bf16[2,1024,16]{1,2,0:T(8,128)(2,1)} %param.18), kind=kLoop, calls=%fused_computation.206 | loop fusion | bytes 131072 | tf_op jit(solution)/shard_map/slice | solution.py:161
  3.6 0.7 broadcast_select_fusion.1
  4.3 3.7 %collective-permute-start.2 = (bf16[8,1024]{1,0:T(8,128)(2,1)S(1)}, bf16[8,1024]{1,0:T(8,128)(2,1)S(1)}, u32[]{:S(2)}, u32[]{:S(2)}) collective-permute-start(bf16[8,1024]{1,0:T(8,128)(2,1)S(1)} %pad_maximum_fusion.1), channel_id=1, source_target_pairs={{0,16},{4,20},{8,24},{12,28},{16,0},{20,4},{24,8},{28,12},{1,17},{... | collective-permute-start | bytes 49160 | tf_op jit(solution)/shard_map/ppermute | solution.py:86
  8.0 1.3 %collective-permute-start.1 = (bf16[8,1024]{1,0:T(8,128)(2,1)S(1)}, bf16[8,1024]{1,0:T(8,128)(2,1)S(1)}, u32[]{:S(2)}, u32[]{:S(2)}) collective-permute-start(bf16[8,1024]{1,0:T(8,128)(2,1)S(1)} %pad_maximum_fusion.1), channel_id=1, source_target_pairs={{0,24},{4,28},{8,0},{12,4},{16,8},{20,12},{24,16},{28,20},{1,25},{... | collective-permute-start | bytes 49160 | tf_op jit(solution)/shard_map/ppermute | solution.py:86
  10.1 1.7 %collective-permute-done.1 = bf16[8,1024]{1,0:T(8,128)(2,1)S(1)} collective-permute-done((bf16[8,1024]{1,0:T(8,128)(2,1)S(1)}, bf16[8,1024]{1,0:T(8,128)(2,1)S(1)}, u32[]{:S(2)}, u32[]{:S(2)}) %collective-permute-start.1) | collective-permute-done | bytes 16416 | tf_op jit(solution)/shard_map/ppermute | solution.py:86
  11.8 3.1 %collective-permute-done.3 = bf16[8,1024]{1,0:T(8,128)(2,1)S(1)} collective-permute-done((bf16[8,1024]{1,0:T(8,128)(2,1)S(1)}, bf16[8,1024]{1,0:T(8,128)(2,1)S(1)}, u32[]{:S(2)}, u32[]{:S(2)}) %collective-permute-start.3) | collective-permute-done | bytes 16416 | tf_op jit(solution)/shard_map/ppermute | solution.py:86
  15.6 1.1 %fusion.18 = f32[4,8,128]{2,1,0:T(8,128)S(1)} fusion(bf16[2,1024,128]{2,1,0:T(8,128)(2,1)} %param.17, f32[1024]{0:T(1024)S(1)} %bitcast.226, bf16[8,8,1024]{2,1,0:T(8,128)(2,1)S(1)} %constant_dynamic-update-slice_fusion, s32[]{:T(128)S(6)} %select_n.125), kind=kOutput, calls=%fused_computation.24 | convolution fusion | flops 8486912 | bytes 348164 | tf_op jit(solution)/shard_map/dot_general | solution.py:172
  17.1 1.5 %collective-permute-start.4 = (f32[8,515]{1,0:T(8,128)S(1)}, f32[8,515]{1,0:T(8,128)S(1)}, u32[]{:S(2)}, u32[]{:S(2)}) collective-permute-start(f32[8,515]{1,0:T(8,128)S(1)} %get-tuple-element.47), channel_id=1, source_target_pairs={{0,1},{1,2},{2,3},{3,0},{4,5},{5,6},{6,7},{7,4},{8,9},{9,10},{10,1... | collective-permute-start | bytes 49448 | tf_op jit(solution)/shard_map/ppermute | solution.py:59
  18.7 1.4 %collective-permute-start.6 = (f32[8,515]{1,0:T(8,128)S(1)}, f32[8,515]{1,0:T(8,128)S(1)}, u32[]{:S(2)}, u32[]{:S(2)}) collective-permute-start(f32[8,515]{1,0:T(8,128)S(1)} %get-tuple-element.48), channel_id=1, source_target_pairs={{0,3},{1,0},{2,1},{3,2},{4,7},{5,4},{6,5},{7,6},{8,11},{9,8},{10,9... | collective-permute-start | bytes 49448 | tf_op jit(solution)/shard_map/ppermute | solution.py:59
  20.1 1.5 %collective-permute-start.5 = (f32[8,515]{1,0:T(8,128)S(1)}, f32[8,515]{1,0:T(8,128)S(1)}, u32[]{:S(2)}, u32[]{:S(2)}) collective-permute-start(f32[8,515]{1,0:T(8,128)S(1)} %get-tuple-element.49), channel_id=1, source_target_pairs={{0,2},{1,3},{2,0},{3,1},{4,6},{5,7},{6,4},{7,5},{8,10},{9,11},{10,... | collective-permute-start | bytes 49448 | tf_op jit(solution)/shard_map/ppermute | solution.py:59
  22.4 1.4 %collective-permute-done.5 = f32[8,515]{1,0:T(8,128)S(1)} collective-permute-done((f32[8,515]{1,0:T(8,128)S(1)}, f32[8,515]{1,0:T(8,128)S(1)}, u32[]{:S(2)}, u32[]{:S(2)}) %collective-permute-start.5) | collective-permute-done | bytes 16512 | tf_op jit(solution)/shard_map/ppermute | solution.py:59
  24.2 1.5 %exponential_reduce_fusion.3 = (f32[8]{0:T(128)S(1)}, f32[8]{0:T(128)S(1)}, f32[8,1]{1,0:T(8,128)S(1)}) fusion(f32[8,1]{1,0:T(8,128)S(1)} %copy.47, f32[]{:T(128)} %bitcast.22, f32[8,2]{1,0:T(8,128)S(1)} %slice_multiply_fusion.9, f32[]{:T(128)} %bitcast.24), kind=kLoop, calls=%fused_computation.185 | loop fusion | flops 112 | bytes 200 | tf_op jit(solution)/shard_map/exp | solution.py:23
  26.7 1.6 %collective-permute-start.7 = (bf16[8,128]{1,0:T(8,128)(2,1)S(1)}, bf16[8,128]{1,0:T(8,128)(2,1)S(1)}, u32[]{:S(2)}, u32[]{:S(2)}) collective-permute-start(bf16[8,128]{1,0:T(8,128)(2,1)S(1)} %get-tuple-element.38), channel_id=1, source_target_pairs={{0,3},{1,0},{2,1},{3,2},{4,7},{5,4},{6,5},{7,6},{8,11},{9,8},{10,9... | collective-permute-start | bytes 6152 | tf_op jit(solution)/shard_map/ppermute | solution.py:46
  28.7 1.5 %collective-permute-start.8 = (bf16[8,128]{1,0:T(8,128)(2,1)S(1)}, bf16[8,128]{1,0:T(8,128)(2,1)S(1)}, u32[]{:S(2)}, u32[]{:S(2)}) collective-permute-start(bf16[8,128]{1,0:T(8,128)(2,1)S(1)} %get-tuple-element.38), channel_id=1, source_target_pairs={{0,2},{1,3},{2,0},{3,1},{4,6},{5,7},{6,4},{7,5},{8,10},{9,11},{10,... | collective-permute-start | bytes 6152 | tf_op jit(solution)/shard_map/ppermute | solution.py:46
  30.3 2.0 %collective-permute-done.8 = bf16[8,128]{1,0:T(8,128)(2,1)S(1)} collective-permute-done((bf16[8,128]{1,0:T(8,128)(2,1)S(1)}, bf16[8,128]{1,0:T(8,128)(2,1)S(1)}, u32[]{:S(2)}, u32[]{:S(2)}) %collective-permute-start.8) | collective-permute-done | bytes 2080 | tf_op jit(solution)/shard_map/ppermute | solution.py:46
  33.0 1.2 %collective-permute-done.10 = bf16[32,1024]{1,0:T(8,128)(2,1)S(1)} collective-permute-done((bf16[32,1024]{1,0:T(8,128)(2,1)S(1)}, bf16[32,1024]{1,0:T(8,128)(2,1)S(1)}, u32[]{:S(2)}, u32[]{:S(2)}) %collective-permute-start.10) | collective-permute-done | bytes 65568 | tf_op jit(solution)/shard_map/ppermute | solution.py:99
  34.4 4.3 %collective-permute-done.11 = bf16[32,1024]{1,0:T(8,128)(2,1)S(1)} collective-permute-done((bf16[32,1024]{1,0:T(8,128)(2,1)S(1)}, bf16[32,1024]{1,0:T(8,128)(2,1)S(1)}, u32[]{:S(2)}, u32[]{:S(2)}) %collective-permute-start.11) | collective-permute-done | bytes 65568 | tf_op jit(solution)/shard_map/ppermute | solution.py:99
  38.8 6.0 %collective-permute-done.12 = bf16[32,1024]{1,0:T(8,128)(2,1)S(1)} collective-permute-done((bf16[32,1024]{1,0:T(8,128)(2,1)S(1)}, bf16[32,1024]{1,0:T(8,128)(2,1)S(1)}, u32[]{:S(2)}, u32[]{:S(2)}) %collective-permute-start.12) | collective-permute-done | bytes 65568 | tf_op jit(solution)/shard_map/ppermute | solution.py:99
  45.3 0.7 copy-done.3
  46.6 1.5 %collective-permute-start.13 = (f32[8,515]{1,0:T(8,128)S(1)}, f32[8,515]{1,0:T(8,128)S(1)}, u32[]{:S(2)}, u32[]{:S(2)}) collective-permute-start(f32[8,515]{1,0:T(8,128)S(1)} %get-tuple-element.44), channel_id=1, source_target_pairs={{0,1},{1,2},{2,3},{3,0},{4,5},{5,6},{6,7},{7,4},{8,9},{9,10},{10,1... | collective-permute-start | bytes 49448 | tf_op jit(solution)/shard_map/ppermute | solution.py:59
  48.2 1.5 %collective-permute-start.15 = (f32[8,515]{1,0:T(8,128)S(1)}, f32[8,515]{1,0:T(8,128)S(1)}, u32[]{:S(2)}, u32[]{:S(2)}) collective-permute-start(f32[8,515]{1,0:T(8,128)S(1)} %get-tuple-element.45), channel_id=1, source_target_pairs={{0,3},{1,0},{2,1},{3,2},{4,7},{5,4},{6,5},{7,6},{8,11},{9,8},{10,9... | collective-permute-start | bytes 49448 | tf_op jit(solution)/shard_map/ppermute | solution.py:59
  49.6 1.1 %collective-permute-start.14 = (f32[8,515]{1,0:T(8,128)S(1)}, f32[8,515]{1,0:T(8,128)S(1)}, u32[]{:S(2)}, u32[]{:S(2)}) collective-permute-start(f32[8,515]{1,0:T(8,128)S(1)} %get-tuple-element.46), channel_id=1, source_target_pairs={{0,2},{1,3},{2,0},{3,1},{4,6},{5,7},{6,4},{7,5},{8,10},{9,11},{10,... | collective-permute-start | bytes 49448 | tf_op jit(solution)/shard_map/ppermute | solution.py:59
  51.9 1.5 %collective-permute-done.14 = f32[8,515]{1,0:T(8,128)S(1)} collective-permute-done((f32[8,515]{1,0:T(8,128)S(1)}, f32[8,515]{1,0:T(8,128)S(1)}, u32[]{:S(2)}, u32[]{:S(2)}) %collective-permute-start.14) | collective-permute-done | bytes 16512 | tf_op jit(solution)/shard_map/ppermute | solution.py:59
  53.7 1.5 %exponential_reduce_fusion.1 = (f32[8]{0:T(128)S(1)}, f32[8]{0:T(128)S(1)}, f32[8,1]{1,0:T(8,128)S(1)}) fusion(f32[8,1]{1,0:T(8,128)S(1)} %copy.52, f32[]{:T(128)} %bitcast.52, f32[8,2]{1,0:T(8,128)S(1)} %slice_multiply_fusion.3, f32[]{:T(128)} %bitcast.54), kind=kLoop, calls=%fused_computation.177 | loop fusion | flops 112 | bytes 200 | tf_op jit(solution)/shard_map/exp | solution.py:23
  56.2 0.8 %collective-permute-start.18 = (bf16[8,128]{1,0:T(8,128)(2,1)S(1)}, bf16[8,128]{1,0:T(8,128)(2,1)S(1)}, u32[]{:S(2)}, u32[]{:S(2)}) collective-permute-start(bf16[8,128]{1,0:T(8,128)(2,1)S(1)} %get-tuple-element.31), channel_id=1, source_target_pairs={{0,1},{1,2},{2,3},{3,0},{4,5},{5,6},{6,7},{7,4},{8,9},{9,10},{10,1... | collective-permute-start | bytes 6152 | tf_op jit(solution)/shard_map/ppermute | solution.py:46
  57.0 0.9 %collective-permute-start.17 = (bf16[8,128]{1,0:T(8,128)(2,1)S(1)}, bf16[8,128]{1,0:T(8,128)(2,1)S(1)}, u32[]{:S(2)}, u32[]{:S(2)}) collective-permute-start(bf16[8,128]{1,0:T(8,128)(2,1)S(1)} %get-tuple-element.31), channel_id=1, source_target_pairs={{0,2},{1,3},{2,0},{3,1},{4,6},{5,7},{6,4},{7,5},{8,10},{9,11},{10,... | collective-permute-start | bytes 6152 | tf_op jit(solution)/shard_map/ppermute | solution.py:46
  57.9 2.3 %collective-permute-start.16 = (bf16[8,128]{1,0:T(8,128)(2,1)S(1)}, bf16[8,128]{1,0:T(8,128)(2,1)S(1)}, u32[]{:S(2)}, u32[]{:S(2)}) collective-permute-start(bf16[8,128]{1,0:T(8,128)(2,1)S(1)} %get-tuple-element.31), channel_id=1, source_target_pairs={{0,3},{1,0},{2,1},{3,2},{4,7},{5,4},{6,5},{7,6},{8,11},{9,8},{10,9... | collective-permute-start | bytes 6152 | tf_op jit(solution)/shard_map/ppermute | solution.py:46
  60.6 1.0 %pad_maximum_fusion = f32[2,8,1,128,128]{4,3,2,1,0:T(8,128)} fusion(f32[1,8,1,128,128]{4,3,2,1,0:T(8,128)S(1)} %get-tuple-element.43, f32[1,8,1,128,128]{4,3,2,1,0:T(8,128)S(1)} %get-tuple-element.42), kind=kLoop, calls=%fused_computation.1 | loop fusion | flops 262144 | bytes 2097152 | tf_op jit(solution)/shard_map/stack | solution.py:222
  63.4 3.8 %collective-permute-start.22 = (bf16[4,1024]{1,0:T(4,128)(2,1)S(1)}, bf16[4,1024]{1,0:T(4,128)(2,1)S(1)}, u32[]{:S(2)}, u32[]{:S(2)}) collective-permute-start(bf16[4,1024]{1,0:T(4,128)(2,1)S(1)} %get-tuple-element.53), channel_id=1, source_target_pairs={{0,24},{4,28},{8,0},{12,4},{16,8},{20,12},{24,16},{28,20},{1,25},{... | collective-permute-start | bytes 24584 | tf_op jit(solution)/shard_map/ppermute | solution.py:117
  67.8 1.1 %collective-permute-done.20 = bf16[4,1024]{1,0:T(4,128)(2,1)S(1)} collective-permute-done((bf16[4,1024]{1,0:T(4,128)(2,1)S(1)}, bf16[4,1024]{1,0:T(4,128)(2,1)S(1)}, u32[]{:S(2)}, u32[]{:S(2)}) %collective-permute-start.20) | collective-permute-done | bytes 8224 | tf_op jit(solution)/shard_map/ppermute | solution.py:117
  68.8 2.9 %collective-permute-done.21 = bf16[4,1024]{1,0:T(4,128)(2,1)S(1)} collective-permute-done((bf16[4,1024]{1,0:T(4,128)(2,1)S(1)}, bf16[4,1024]{1,0:T(4,128)(2,1)S(1)}, u32[]{:S(2)}, u32[]{:S(2)}) %collective-permute-start.21) | collective-permute-done | bytes 8224 | tf_op jit(solution)/shard_map/ppermute | solution.py:117
  (118 shorter events, 13.3 us)
Async XLA Ops:
  0.6 14.6 %copy-start.1 = (bf16[2,1024,128]{2,1,0:T(8,128)(2,1)S(1)}, bf16[2,1024,128]{2,1,0:T(8,128)(2,1)}, u32[]{:S(2)}) copy-start(bf16[2,1024,128]{2,1,0:T(8,128)(2,1)} %param.15) | copy-start | bytes 1572868
  0.6 2.9 %collective-permute-start = (bf16[4,1024]{1,0:T(4,128)(2,1)}, bf16[4,1024]{1,0:T(4,128)(2,1)S(1)}, u32[]{:S(2)}, u32[]{:S(2)}) collective-permute-start(bf16[4,1024]{1,0:T(4,128)(2,1)} %param.12), channel_id=1, source_target_pairs={{0,4},{4,0},{8,12},{12,8},{16,20},{20,16},{24,28},{28,24},{1,5},{5... | collective-permute-start | bytes 24584 | tf_op jit(solution)/shard_map/ppermute | solution.py:72
  2.6 12.7 %copy-start.2 = (bf16[2,1024,128]{2,1,0:T(8,128)(2,1)S(1)}, bf16[2,1024,128]{2,1,0:T(8,128)(2,1)}, u32[]{:S(2)}) copy-start(bf16[2,1024,128]{2,1,0:T(8,128)(2,1)} %param.16) | copy-start | bytes 1572868
  4.3 7.5 %collective-permute-start.2 = (bf16[8,1024]{1,0:T(8,128)(2,1)S(1)}, bf16[8,1024]{1,0:T(8,128)(2,1)S(1)}, u32[]{:S(2)}, u32[]{:S(2)}) collective-permute-start(bf16[8,1024]{1,0:T(8,128)(2,1)S(1)} %pad_maximum_fusion.1), channel_id=1, source_target_pairs={{0,16},{4,20},{8,24},{12,28},{16,0},{20,4},{24,8},{28,12},{1,17},{... | collective-permute-start | bytes 49160 | tf_op jit(solution)/shard_map/ppermute | solution.py:86
  8.0 3.7 %collective-permute-start.1 = (bf16[8,1024]{1,0:T(8,128)(2,1)S(1)}, bf16[8,1024]{1,0:T(8,128)(2,1)S(1)}, u32[]{:S(2)}, u32[]{:S(2)}) collective-permute-start(bf16[8,1024]{1,0:T(8,128)(2,1)S(1)} %pad_maximum_fusion.1), channel_id=1, source_target_pairs={{0,24},{4,28},{8,0},{12,4},{16,8},{20,12},{24,16},{28,20},{1,25},{... | collective-permute-start | bytes 49160 | tf_op jit(solution)/shard_map/ppermute | solution.py:86
  9.4 5.5 %collective-permute-start.3 = (bf16[8,1024]{1,0:T(8,128)(2,1)S(1)}, bf16[8,1024]{1,0:T(8,128)(2,1)S(1)}, u32[]{:S(2)}, u32[]{:S(2)}) collective-permute-start(bf16[8,1024]{1,0:T(8,128)(2,1)S(1)} %pad_maximum_fusion.1), channel_id=1, source_target_pairs={{0,8},{4,12},{8,16},{12,20},{16,24},{20,28},{24,0},{28,4},{1,9},{5... | collective-permute-start | bytes 49160 | tf_op jit(solution)/shard_map/ppermute | solution.py:86
  15.0 1.7 %copy-start.4 = (bf16[2,1024,128]{2,1,0:T(8,128)(2,1)S(1)}, bf16[2,1024,128]{2,1,0:T(8,128)(2,1)}, u32[]{:S(2)}) copy-start(bf16[2,1024,128]{2,1,0:T(8,128)(2,1)} %param.14) | copy-start | bytes 1572868
  15.0 6.6 %copy-start.7 = (f32[2,2,1]{1,2,0:T(1,128)S(1)}, f32[2,2,1]{1,2,0:T(1,128)}, u32[]{:S(2)}) copy-start(f32[2,2,1]{1,2,0:T(1,128)} %param.19) | copy-start | bytes 52
  15.1 11.1 %copy-start = (f32[2,8,1,128,128]{4,3,2,1,0:T(8,128)S(1)}, f32[2,8,1,128,128]{4,3,2,1,0:T(8,128)}, u32[]{:S(2)}) copy-start(f32[2,8,1,128,128]{4,3,2,1,0:T(8,128)} %param.21) | copy-start | bytes 3145732
  17.0 8.7 %copy-start.6 = (f32[2,8,1,128]{3,2,1,0:T(1,128)S(1)}, f32[2,8,1,128]{3,2,1,0:T(1,128)}, u32[]{:S(2)}) copy-start(f32[2,8,1,128]{3,2,1,0:T(1,128)} %param.22) | copy-start | bytes 24580
  17.1 15.7 %copy-start.5 = (bf16[2,128,1024]{2,1,0:T(8,128)(2,1)S(1)}, bf16[2,128,1024]{2,1,0:T(8,128)(2,1)}, u32[]{:S(2)}) copy-start(bf16[2,128,1024]{2,1,0:T(8,128)(2,1)} %param.20) | copy-start | bytes 1572868
  17.1 5.2 %collective-permute-start.4 = (f32[8,515]{1,0:T(8,128)S(1)}, f32[8,515]{1,0:T(8,128)S(1)}, u32[]{:S(2)}, u32[]{:S(2)}) collective-permute-start(f32[8,515]{1,0:T(8,128)S(1)} %get-tuple-element.47), channel_id=1, source_target_pairs={{0,1},{1,2},{2,3},{3,0},{4,5},{5,6},{6,7},{7,4},{8,9},{9,10},{10,1... | collective-permute-start | bytes 49448 | tf_op jit(solution)/shard_map/ppermute | solution.py:59
  18.7 3.8 %collective-permute-start.6 = (f32[8,515]{1,0:T(8,128)S(1)}, f32[8,515]{1,0:T(8,128)S(1)}, u32[]{:S(2)}, u32[]{:S(2)}) collective-permute-start(f32[8,515]{1,0:T(8,128)S(1)} %get-tuple-element.48), channel_id=1, source_target_pairs={{0,3},{1,0},{2,1},{3,2},{4,7},{5,4},{6,5},{7,6},{8,11},{9,8},{10,9... | collective-permute-start | bytes 49448 | tf_op jit(solution)/shard_map/ppermute | solution.py:59
  20.1 3.8 %collective-permute-start.5 = (f32[8,515]{1,0:T(8,128)S(1)}, f32[8,515]{1,0:T(8,128)S(1)}, u32[]{:S(2)}, u32[]{:S(2)}) collective-permute-start(f32[8,515]{1,0:T(8,128)S(1)} %get-tuple-element.49), channel_id=1, source_target_pairs={{0,2},{1,3},{2,0},{3,1},{4,6},{5,7},{6,4},{7,5},{8,10},{9,11},{10,... | collective-permute-start | bytes 49448 | tf_op jit(solution)/shard_map/ppermute | solution.py:59
  26.7 3.6 %collective-permute-start.7 = (bf16[8,128]{1,0:T(8,128)(2,1)S(1)}, bf16[8,128]{1,0:T(8,128)(2,1)S(1)}, u32[]{:S(2)}, u32[]{:S(2)}) collective-permute-start(bf16[8,128]{1,0:T(8,128)(2,1)S(1)} %get-tuple-element.38), channel_id=1, source_target_pairs={{0,3},{1,0},{2,1},{3,2},{4,7},{5,4},{6,5},{7,6},{8,11},{9,8},{10,9... | collective-permute-start | bytes 6152 | tf_op jit(solution)/shard_map/ppermute | solution.py:46
  28.2 4.5 %collective-permute-start.9 = (bf16[8,128]{1,0:T(8,128)(2,1)S(1)}, bf16[8,128]{1,0:T(8,128)(2,1)S(1)}, u32[]{:S(2)}, u32[]{:S(2)}) collective-permute-start(bf16[8,128]{1,0:T(8,128)(2,1)S(1)} %get-tuple-element.38), channel_id=1, source_target_pairs={{0,1},{1,2},{2,3},{3,0},{4,5},{5,6},{6,7},{7,4},{8,9},{9,10},{10,1... | collective-permute-start | bytes 6152 | tf_op jit(solution)/shard_map/ppermute | solution.py:46
  28.7 3.6 %collective-permute-start.8 = (bf16[8,128]{1,0:T(8,128)(2,1)S(1)}, bf16[8,128]{1,0:T(8,128)(2,1)S(1)}, u32[]{:S(2)}, u32[]{:S(2)}) collective-permute-start(bf16[8,128]{1,0:T(8,128)(2,1)S(1)} %get-tuple-element.38), channel_id=1, source_target_pairs={{0,2},{1,3},{2,0},{3,1},{4,6},{5,7},{6,4},{7,5},{8,10},{9,11},{10,... | collective-permute-start | bytes 6152 | tf_op jit(solution)/shard_map/ppermute | solution.py:46
  32.9 1.3 %collective-permute-start.10 = (bf16[32,1024]{1,0:T(8,128)(2,1)S(1)}, bf16[32,1024]{1,0:T(8,128)(2,1)S(1)}, u32[]{:S(2)}, u32[]{:S(2)}) collective-permute-start(bf16[32,1024]{1,0:T(8,128)(2,1)S(1)} %get-tuple-element.73), channel_id=1, source_target_pairs={{0,4},{4,0},{8,12},{12,8},{16,20},{20,16},{24,28},{28,24},{1,5},{5... | collective-permute-start | bytes 196616 | tf_op jit(solution)/shard_map/ppermute | solution.py:99
  34.3 4.3 %collective-permute-start.11 = (bf16[32,1024]{1,0:T(8,128)(2,1)S(1)}, bf16[32,1024]{1,0:T(8,128)(2,1)S(1)}, u32[]{:S(2)}, u32[]{:S(2)}) collective-permute-start(bf16[32,1024]{1,0:T(8,128)(2,1)S(1)} %fusion.40), channel_id=1, source_target_pairs={{0,8},{4,12},{8,0},{12,4},{16,24},{20,28},{24,16},{28,20},{1,9},{5... | collective-permute-start | bytes 196616 | tf_op jit(solution)/shard_map/ppermute | solution.py:99
  38.6 6.1 %collective-permute-start.12 = (bf16[32,1024]{1,0:T(8,128)(2,1)S(1)}, bf16[32,1024]{1,0:T(8,128)(2,1)S(1)}, u32[]{:S(2)}, u32[]{:S(2)}) collective-permute-start(bf16[32,1024]{1,0:T(8,128)(2,1)S(1)} %fusion.46), channel_id=1, source_target_pairs={{0,24},{4,28},{8,16},{12,20},{16,8},{20,12},{24,0},{28,4},{1,25},{... | collective-permute-start | bytes 196616 | tf_op jit(solution)/shard_map/ppermute | solution.py:99
  44.9 1.0 %copy-start.3 = (bf16[2,1024,128]{2,1,0:T(8,128)(2,1)S(1)}, bf16[2,1024,128]{2,1,0:T(8,128)(2,1)}, u32[]{:S(2)}) copy-start(bf16[2,1024,128]{2,1,0:T(8,128)(2,1)} %param.17) | copy-start | bytes 1572868
  46.6 4.7 %collective-permute-start.13 = (f32[8,515]{1,0:T(8,128)S(1)}, f32[8,515]{1,0:T(8,128)S(1)}, u32[]{:S(2)}, u32[]{:S(2)}) collective-permute-start(f32[8,515]{1,0:T(8,128)S(1)} %get-tuple-element.44), channel_id=1, source_target_pairs={{0,1},{1,2},{2,3},{3,0},{4,5},{5,6},{6,7},{7,4},{8,9},{9,10},{10,1... | collective-permute-start | bytes 49448 | tf_op jit(solution)/shard_map/ppermute | solution.py:59
  48.2 3.8 %collective-permute-start.15 = (f32[8,515]{1,0:T(8,128)S(1)}, f32[8,515]{1,0:T(8,128)S(1)}, u32[]{:S(2)}, u32[]{:S(2)}) collective-permute-start(f32[8,515]{1,0:T(8,128)S(1)} %get-tuple-element.45), channel_id=1, source_target_pairs={{0,3},{1,0},{2,1},{3,2},{4,7},{5,4},{6,5},{7,6},{8,11},{9,8},{10,9... | collective-permute-start | bytes 49448 | tf_op jit(solution)/shard_map/ppermute | solution.py:59
  49.6 3.8 %collective-permute-start.14 = (f32[8,515]{1,0:T(8,128)S(1)}, f32[8,515]{1,0:T(8,128)S(1)}, u32[]{:S(2)}, u32[]{:S(2)}) collective-permute-start(f32[8,515]{1,0:T(8,128)S(1)} %get-tuple-element.46), channel_id=1, source_target_pairs={{0,2},{1,3},{2,0},{3,1},{4,6},{5,7},{6,4},{7,5},{8,10},{9,11},{10,... | collective-permute-start | bytes 49448 | tf_op jit(solution)/shard_map/ppermute | solution.py:59
  56.2 5.5 %collective-permute-start.18 = (bf16[8,128]{1,0:T(8,128)(2,1)S(1)}, bf16[8,128]{1,0:T(8,128)(2,1)S(1)}, u32[]{:S(2)}, u32[]{:S(2)}) collective-permute-start(bf16[8,128]{1,0:T(8,128)(2,1)S(1)} %get-tuple-element.31), channel_id=1, source_target_pairs={{0,1},{1,2},{2,3},{3,0},{4,5},{5,6},{6,7},{7,4},{8,9},{9,10},{10,1... | collective-permute-start | bytes 6152 | tf_op jit(solution)/shard_map/ppermute | solution.py:46
  57.0 4.7 %collective-permute-start.17 = (bf16[8,128]{1,0:T(8,128)(2,1)S(1)}, bf16[8,128]{1,0:T(8,128)(2,1)S(1)}, u32[]{:S(2)}, u32[]{:S(2)}) collective-permute-start(bf16[8,128]{1,0:T(8,128)(2,1)S(1)} %get-tuple-element.31), channel_id=1, source_target_pairs={{0,2},{1,3},{2,0},{3,1},{4,6},{5,7},{6,4},{7,5},{8,10},{9,11},{10,... | collective-permute-start | bytes 6152 | tf_op jit(solution)/shard_map/ppermute | solution.py:46
  57.9 3.8 %collective-permute-start.16 = (bf16[8,128]{1,0:T(8,128)(2,1)S(1)}, bf16[8,128]{1,0:T(8,128)(2,1)S(1)}, u32[]{:S(2)}, u32[]{:S(2)}) collective-permute-start(bf16[8,128]{1,0:T(8,128)(2,1)S(1)} %get-tuple-element.31), channel_id=1, source_target_pairs={{0,3},{1,0},{2,1},{3,2},{4,7},{5,4},{6,5},{7,6},{8,11},{9,8},{10,9... | collective-permute-start | bytes 6152 | tf_op jit(solution)/shard_map/ppermute | solution.py:46
  62.0 1.3 %collective-permute-start.19 = (bf16[4,4,1024]{2,1,0:T(4,128)(2,1)S(1)}, bf16[4,4,1024]{2,1,0:T(4,128)(2,1)S(1)}, u32[]{:S(2)}, u32[]{:S(2)}) collective-permute-start(bf16[4,4,1024]{2,1,0:T(4,128)(2,1)S(1)} %fusion.47), channel_id=1, source_target_pairs={{0,4},{4,0},{8,12},{12,8},{16,20},{20,16},{24,28},{28,24},{1,5},{5... | collective-permute-start | bytes 98312 | tf_op jit(solution)/shard_map/ppermute | solution.py:72
  63.3 5.5 %collective-permute-start.20 = (bf16[4,1024]{1,0:T(4,128)(2,1)S(1)}, bf16[4,1024]{1,0:T(4,128)(2,1)S(1)}, u32[]{:S(2)}, u32[]{:S(2)}) collective-permute-start(bf16[4,1024]{1,0:T(4,128)(2,1)S(1)} %get-tuple-element.52), channel_id=1, source_target_pairs={{0,8},{4,12},{8,16},{12,20},{16,24},{20,28},{24,0},{28,4},{1,9},{5... | collective-permute-start | bytes 24584 | tf_op jit(solution)/shard_map/ppermute | solution.py:117
  63.4 5.4 %collective-permute-start.22 = (bf16[4,1024]{1,0:T(4,128)(2,1)S(1)}, bf16[4,1024]{1,0:T(4,128)(2,1)S(1)}, u32[]{:S(2)}, u32[]{:S(2)}) collective-permute-start(bf16[4,1024]{1,0:T(4,128)(2,1)S(1)} %get-tuple-element.53), channel_id=1, source_target_pairs={{0,24},{4,28},{8,0},{12,4},{16,8},{20,12},{24,16},{28,20},{1,25},{... | collective-permute-start | bytes 24584 | tf_op jit(solution)/shard_map/ppermute | solution.py:117
  67.2 4.5 %collective-permute-start.21 = (bf16[4,1024]{1,0:T(4,128)(2,1)S(1)}, bf16[4,1024]{1,0:T(4,128)(2,1)S(1)}, u32[]{:S(2)}, u32[]{:S(2)}) collective-permute-start(bf16[4,1024]{1,0:T(4,128)(2,1)S(1)} %get-tuple-element.54), channel_id=1, source_target_pairs={{0,16},{4,20},{8,24},{12,28},{16,0},{20,4},{24,8},{28,12},{1,17},{... | collective-permute-start | bytes 24584 | tf_op jit(solution)/shard_map/ppermute | solution.py:117
